TPU v7x, 256 devices: a whole 4x4x8 slice. The times are simulated.
256 devices in a mesh: ep: 64 (over z, y, core), tp: 4 (over x).
Axes of the slice: x: 4, y: 4, z: 8, core: 2. Of those that a mesh axis runs over, the one named last changes fastest.
Arguments:
- queries: bfloat16 [16384, 8, 128], P('ep', 'tp'), may hold values from -6 to 6
- keys: bfloat16 [16384, 4, 128], P('ep', 'tp'), may hold values from -6 to 6
- values: bfloat16 [16384, 4, 128], P('ep', 'tp'), may hold values from -6 to 6
- query_gain: float32 [128], replicated, may hold values from 1.5 to 7
- key_gain: float32 [128], replicated, may hold values from 1.5 to 7
- routed_rows: bfloat16 [32768, 2048], P(('ep', 'tp')), may hold values from -6 to 6
- mixture_gain: float32 [2048], replicated, may hold values from 0.1 to 1.9
- expert_index: int32 [32768, 2], P(('ep', 'tp')), may hold values from 0 to 63, as said below
- route_weights: float32 [32768, 2], P(('ep', 'tp')), may hold values from 0.1 to 1
- expert_gate: bfloat16 [64, 768, 2048], P('ep', 'tp'), may hold values from -0.125 to 0.125
- expert_up: bfloat16 [64, 768, 2048], P('ep', 'tp'), may hold values from -0.125 to 0.125
- expert_down: bfloat16 [64, 768, 2048], P('ep', 'tp'), may hold values from -0.21875 to 0.21875
Outputs:
- attended: bfloat16 [16384, 8, 128], P('ep', 'tp')
- combined: bfloat16 [32768, 2048], P(('ep', 'tp'))
Inputs may be any that keep to these rules, and one draw needn't show every extreme that they name: `expert_index`: each row names 2 different experts that lie in one group of 16 consecutive experts. In every aligned block of 128 rows (the rows of one device) no expert is named by more than 8 rows, and the experts of one group, the same group in all blocks, are each named by exactly 8 rows.
All inputs are finite; a program needn't handle non-finite values.
Results may differ from a plain program's by a relative error of at most 0.011.
The roundings to bfloat16 on the way count: a program that leaves them out, or rounds other values in their place, can miss the bound.
Values may be sent and summed in bfloat16 or wider, within the bound.
A program may use at most 128 MiB of HBM per device.

v0:
```python
import jax
import jax.numpy as jnp
from jax import lax
from jax.sharding import PartitionSpec as P

GROUPS = 4
GRID_W = 64


epsilon = 1e-06
rotary_base = 10000.0
floor_value = -1e30


def side_by_side(arrays, axis, dim, along):
    ends, at = ([], 0)
    for a in arrays[:-1]:
        at += a.shape[along]
        ends.append(at)
    both = jnp.concatenate(arrays, axis=along)
    return tuple(jnp.split(lax.all_gather(both, axis, axis=dim, tiled=True), ends, axis=along))


def in_blocks(value, dim, devices):
    dims = value.shape
    blocks = value.reshape(*dims[:dim], devices, dims[dim] // devices, *dims[dim + 1 :])
    return jnp.moveaxis(blocks, dim, 0)


def cut_rows(length, count):
    unit = 8 if length >= 8 * count else 1
    return [length // unit * k // count * unit for k in range(1, count)]


def joined_along(blocks, dim):
    blocks = jnp.moveaxis(blocks, 0, dim)
    dims = blocks.shape
    return blocks.reshape(*dims[:dim], dims[dim] * dims[dim + 1], *dims[dim + 2 :])


def exchange_in_pieces(value, axis, pieces, split_dim, concat_dim):
    blocks = in_blocks(value, split_dim, lax.axis_size(axis))
    widest = max(range(1, max(2, blocks.ndim - 1)), key=lambda d: blocks.shape[d])
    outs = []
    for section in jnp.split(blocks, cut_rows(blocks.shape[widest], pieces), axis=widest):
        if section.size:
            outs.append(lax.all_to_all(section, axis, split_axis=0, concat_axis=0, tiled=True))
    return joined_along(jnp.concatenate(outs, axis=widest), concat_dim)


def normalize(inputs, gain_vector):
    values_f = inputs.astype(jnp.float32)
    return (
        values_f
        * lax.rsqrt(jnp.mean(values_f * values_f, axis=-1, keepdims=True) + epsilon)
        * gain_vector
    )


def rotate(normed, positions):
    head_width = normed.shape[-1]
    quarter = head_width // 4
    frequency = rotary_base ** (-jnp.arange(quarter, dtype=jnp.float32) / quarter)
    grid_row = (positions // GRID_W).astype(jnp.float32)
    grid_col = (positions % GRID_W).astype(jnp.float32)
    angles = jnp.concatenate(
        [grid_row[:, None] * frequency, grid_col[:, None] * frequency], axis=-1
    )[:, None, :]
    cosine_table = jnp.cos(angles)
    sine_table = jnp.sin(angles)
    lower_half, upper_half = jnp.split(normed, 2, axis=-1)
    turned = jnp.concatenate(
        [
            lower_half * cosine_table - upper_half * sine_table,
            lower_half * sine_table + upper_half * cosine_table,
        ],
        axis=-1,
    )
    return turned.astype(jnp.bfloat16)


def merge_block(running, key_block, grouped, factor):
    maxima, totals, weighted = running
    block_keys, block_values = key_block
    scores = (
        jnp.einsum("tkgd,skd->kgts", grouped, block_keys, preferred_element_type=jnp.float32)
        * factor
    )
    local_max = jnp.max(scores, axis=-1)
    shifted = jnp.exp(scores - local_max[..., None])
    block_mass = jnp.sum(shifted, axis=-1)
    block_sum = jnp.einsum(
        "kgts,skd->kgtd",
        shifted.astype(jnp.bfloat16),
        block_values,
        preferred_element_type=jnp.float32,
    )
    top_max = jnp.maximum(maxima, local_max)
    keep_old = jnp.exp(maxima - top_max)
    keep_new = jnp.exp(local_max - top_max)
    return (
        top_max,
        totals * keep_old + block_mass * keep_new,
        weighted * keep_old[..., None] + block_sum * keep_new[..., None],
    )


def settle(partial_value):
    rounded = lax.optimization_barrier(partial_value.astype(jnp.bfloat16))
    return rounded.astype(jnp.float32)


def on_device(
    queries,
    keys,
    values,
    query_gain,
    key_gain,
    routed_rows,
    mixture_gain,
    expert_index,
    route_weights,
    expert_gate,
    expert_up,
    expert_down,
):
    length = queries.shape[0]
    head_width = queries.shape[2]
    kv_heads = keys.shape[1]
    group_size = queries.shape[1] // kv_heads
    positions = lax.axis_index("ep") * length + jnp.arange(length, dtype=jnp.int32)
    turned_queries = rotate(normalize(queries, query_gain), positions)
    turned_keys = rotate(normalize(keys, key_gain), positions)
    grouped = turned_queries.reshape(length, kv_heads, group_size, head_width)
    factor = head_width ** (-0.5)
    initial = (
        jnp.full((kv_heads, group_size, length), floor_value, jnp.float32),
        jnp.zeros((kv_heads, group_size, length), jnp.float32),
        jnp.zeros((kv_heads, group_size, length, head_width), jnp.float32),
    )
    running = initial
    key_piece, value_piece = side_by_side((turned_keys, values), "ep", 0, 1)
    shards = key_piece.shape[0] // length
    stacked = (
        key_piece.reshape(shards, length, kv_heads, head_width),
        value_piece.reshape(shards, length, kv_heads, head_width),
    )

    def one_block(running_state, key_block):
        return (merge_block(running_state, key_block, grouped, factor), None)

    running, unused = lax.scan(one_block, running, stacked)
    maxima, totals, weighted = running
    attended = (weighted / totals[..., None]).transpose(2, 0, 1, 3)
    attended = attended.reshape(length, kv_heads * group_size, head_width).astype(jnp.bfloat16)
    rows_here = routed_rows.shape[0]
    model_width = routed_rows.shape[1]
    normed_rows = normalize(routed_rows, mixture_gain).astype(jnp.bfloat16)
    ep_count = lax.axis_size("ep")
    local_experts = expert_gate.shape[0]
    experts_all = local_experts * ep_count
    capacity = rows_here // (experts_all // GROUPS)
    flat_ids = expert_index.reshape(-1)
    onehot = (flat_ids[:, None] == jnp.arange(experts_all, dtype=jnp.int32)[None, :]).astype(
        jnp.int32
    )
    earlier = jnp.cumsum(onehot, axis=0) - onehot
    slot_numbers = jnp.sum(earlier * onehot, axis=1)
    places = (
        flat_ids // local_experts * capacity + slot_numbers
    ) * local_experts + flat_ids % local_experts
    owners = jnp.arange(flat_ids.shape[0], dtype=jnp.int32) // expert_index.shape[1]
    source = (
        jnp.full((ep_count * capacity * local_experts,), rows_here, jnp.int32)
        .at[places]
        .set(owners)
    )
    padded = jnp.concatenate([normed_rows, jnp.zeros((1, model_width), jnp.bfloat16)], axis=0)
    outgoing = padded[source].reshape(ep_count * capacity, local_experts, model_width)
    arrived = lax.all_to_all(outgoing, "ep", split_axis=0, concat_axis=0, tiled=True)
    part_width = expert_gate.shape[1]
    running = jnp.zeros(arrived.shape, jnp.float32)
    gate_piece, up_piece, down_piece = side_by_side(
        (expert_gate, expert_up, expert_down), "tp", 1, 0
    )
    for block_index in range(gate_piece.shape[1] // part_width):
        lower_col = block_index * part_width
        gate_block = lax.slice_in_dim(gate_piece, lower_col, lower_col + part_width, axis=1)
        up_block = lax.slice_in_dim(up_piece, lower_col, lower_col + part_width, axis=1)
        down_block = lax.slice_in_dim(down_piece, lower_col, lower_col + part_width, axis=1)
        gate_values = jnp.einsum(
            "rxd,xfd->rxf", arrived, gate_block, preferred_element_type=jnp.float32
        )
        up_values = jnp.einsum(
            "rxd,xfd->rxf", arrived, up_block, preferred_element_type=jnp.float32
        )
        hidden = (jax.nn.silu(gate_values) * up_values).astype(jnp.bfloat16)
        running = running + settle(
            jnp.einsum("rxf,xfd->rxd", hidden, down_block, preferred_element_type=jnp.float32)
        )
    results = running.astype(jnp.bfloat16)
    returned = exchange_in_pieces(results, "ep", 2, 0, 0)
    picked = returned.reshape(-1, model_width)[places].reshape(
        rows_here, expert_index.shape[1], model_width
    )
    combined = jnp.sum(picked.astype(jnp.float32) * route_weights[..., None], axis=1).astype(
        jnp.bfloat16
    )
    return (attended, combined)


def solution(mesh):
    placed = (
        P("ep", "tp", None),
        P("ep", "tp", None),
        P("ep", "tp", None),
        P(),
        P(),
        P(("ep", "tp"), None),
        P(),
        P(("ep", "tp"), None),
        P(("ep", "tp"), None),
        P("ep", "tp", None),
        P("ep", "tp", None),
        P("ep", "tp", None),
    )
    return jax.shard_map(
        on_device,
        mesh=mesh,
        in_specs=placed,
        out_specs=(P("ep", "tp", None), P(("ep", "tp"), None)),
        check_vma=False,
    )
```

profile of v0, /device:TPU:2, one launch (start us, length us, event | category | flops | bytes accessed | tf_op | source)
XLA Modules:
  0.0 408.1 jit_solution(8240076005670327676)
XLA Ops:
  7.2 3.3 pad_maximum_fusion
  15.9 1.4 scatter_custom_fusion
  17.4 2.5 gather_fusion
  20.4 3.0 reduce.5
  23.3 4.9 %reshape.509 = bf16[64,2,8192]{2,1,0:T(2,128)(2,1)} reshape(bf16[512,2048]{1,0:T(8,128)(2,1)} %reduce.5) | data formatting | bytes 4194304
  28.2 63.6 %all_to_all.15 = bf16[64,2,8192]{2,1,0:T(2,128)(2,1)S(1)} all-to-all(bf16[64,2,8192]{2,1,0:T(2,128)(2,1)} %reshape.509), channel_id=1, replica_groups=mesh['ep'=64,'tp'=4] {'ep'}, dimensions={0} | all-to-all | bytes 4194304 | tf_op jit(solution)/shard_map/all_to_all | solution.py:180
  91.8 6.8 %reshape.510 = bf16[512,1,2048]{2,1,0:T(2,128)(2,1)} reshape(bf16[64,2,8192]{2,1,0:T(2,128)(2,1)S(1)} %all_to_all.15) | data formatting | bytes 4194304
  98.6 3.5 copy.69
  102.1 6.1 %all-gather.5.cloned.1.call-done = bf16[3,768,2048]{2,1,0:T(8,128)(2,1)} async-done(((bf16[3,192,2048]{2,1,0:T(8,128)(2,1)}), bf16[3,768,2048]{2,1,0:T(8,128)(2,1)}) %all-gather.5.cloned.1.call-update) | async-done | bytes 9437200 | tf_op jit(solution)/shard_map/all_gather | solution.py:21
  108.2 2.0 fusion.39
  110.1 4.3 %fusion.19 = bf16[512,1,2048]{0,2,1:T(8,128)(2,1)} fusion(bf16[3,768,2048]{2,1,0:T(8,128)(2,1)} %all-gather.5.cloned.1.call-done, bf16[512,1,2048]{2,0,1:T(8,128)(2,1)S(1)} %copy.69, f32[512,1,192]{0,2,1:T(8,128)S(1)} %fusion.39), kind=kOutput, calls=%fused_computation.36 | convolution fusion | flops 806944768 | bytes 6160384 | tf_op jit(solution)/shard_map/rxf,xfd->rxd/dot_general | solution.py:199
  114.4 2.0 fusion.48
  116.4 4.3 %fusion.20 = bf16[512,1,2048]{0,2,1:T(8,128)(2,1)} fusion(bf16[3,768,2048]{2,1,0:T(8,128)(2,1)} %all-gather.5.cloned.1.call-done, bf16[512,1,2048]{2,0,1:T(8,128)(2,1)S(1)} %copy.69, f32[512,1,192]{0,2,1:T(8,128)S(1)} %fusion.48), kind=kOutput, calls=%fused_computation.37 | convolution fusion | flops 806944768 | bytes 6160384 | tf_op jit(solution)/shard_map/rxf,xfd->rxd/dot_general | solution.py:199
  120.7 2.0 fusion.57
  122.7 4.3 %fusion.21 = bf16[512,1,2048]{0,2,1:T(8,128)(2,1)} fusion(bf16[3,768,2048]{2,1,0:T(8,128)(2,1)} %all-gather.5.cloned.1.call-done, bf16[512,1,2048]{2,0,1:T(8,128)(2,1)S(1)} %copy.69, f32[512,1,192]{0,2,1:T(8,128)S(1)} %fusion.57), kind=kOutput, calls=%fused_computation.38 | convolution fusion | flops 806944768 | bytes 6160384 | tf_op jit(solution)/shard_map/rxf,xfd->rxd/dot_general | solution.py:199
  127.0 2.0 fusion.66
  129.0 4.3 %fusion.22 = bf16[512,1,2048]{0,2,1:T(8,128)(2,1)} fusion(bf16[3,768,2048]{2,1,0:T(8,128)(2,1)} %all-gather.5.cloned.1.call-done, bf16[512,1,2048]{2,0,1:T(8,128)(2,1)S(1)} %copy.69, f32[512,1,192]{0,2,1:T(8,128)S(1)} %fusion.66), kind=kOutput, calls=%fused_computation.39 | convolution fusion | flops 806944768 | bytes 6160384 | tf_op jit(solution)/shard_map/rxf,xfd->rxd/dot_general | solution.py:199
  133.3 4.6 %add_convert_fusion = bf16[512,1,2048]{0,2,1:T(8,128)(2,1)S(1)} fusion(bf16[512,1,2048]{0,2,1:T(8,128)(2,1)} %fusion.22, bf16[512,1,2048]{0,2,1:T(8,128)(2,1)} %fusion.21, bf16[512,1,2048]{0,2,1:T(8,128)(2,1)} %fusion.20, bf16[512,1,2048]{0,2,1:T(8,128)(2,1)} %fusion.19), kind=kLoop, calls=%fused_computation.31 | loop fusion | flops 8388608 | bytes 10485760 | tf_op jit(solution)/shard_map/convert_element_type | solution.py:201
  137.9 2.5 copy.63
  140.4 4.4 %slice_bitcast_fusion.1 = (bf16[64,4,1,2048]{3,1,2,0:T(4,128)(2,1)S(1)}, bf16[64,4,1,2048]{3,1,2,0:T(4,128)(2,1)}) fusion(bf16[64,8,1,2048]{3,1,0,2:T(8,128)(2,1)} %bitcast.312), kind=kLoop, calls=%fused_computation.85 | loop fusion | bytes 4194304 | tf_op jit(solution)/shard_map/split | solution.py:45
  144.8 47.4 %all_to_all.16 = bf16[64,4,1,2048]{3,1,2,0:T(4,128)(2,1)S(1)} all-to-all(bf16[64,4,1,2048]{3,1,2,0:T(4,128)(2,1)S(1)} %get-tuple-element.90), channel_id=1, replica_groups=mesh['ep'=64,'tp'=4] {'ep'}, dimensions={0} | all-to-all | bytes 2097152 | tf_op jit(solution)/shard_map/all_to_all | solution.py:47
  192.2 6.6 %all-to-all-start.2 = ((bf16[64,4,1,2048]{3,1,2,0:T(4,128)(2,1)}), bf16[64,4,1,2048]{3,1,2,0:T(4,128)(2,1)}, u32[]{:S(2)}, u32[]{:S(2)}) async-start(bf16[64,4,1,2048]{3,1,2,0:T(4,128)(2,1)} %get-tuple-element.91), calls=%async_computation.2 | async-start | bytes 2097152 | tf_op jit(solution)/shard_map/all_to_all | solution.py:47
  200.8 27.4 %all-to-all-done.2 = bf16[64,4,1,2048]{3,1,2,0:T(4,128)(2,1)} async-done(((bf16[64,4,1,2048]{3,1,2,0:T(4,128)(2,1)}), bf16[64,4,1,2048]{3,1,2,0:T(4,128)(2,1)}, u32[]{:S(2)}, u32[]{:S(2)}) %all-to-all-start.2) | async-done | bytes 1048608 | tf_op jit(solution)/shard_map/all_to_all | solution.py:47
  228.2 2.3 maximum_bitcast_fusion
  230.5 1.4 gather_fusion.1
  231.9 1.3 reshape.474
  233.2 4.8 %multiply_reduce_fusion = bf16[128,2048]{1,0:T(8,128)(2,1)} fusion(f32[128,2,2048]{2,1,0:T(2,128)S(1)} %reshape.474, f32[128,2]{1,0:T(8,128)} %copy.66), kind=kLoop, calls=%fused_computation.58 | loop fusion | flops 786432 | bytes 2622464 | tf_op jit(solution)/shard_map/reduce_sum | solution.py:206
  238.0 5.7 %fusion.161 = (bf16[16384,1,128]{2,0,1:T(8,128)(2,1)}, bf16[16384,1,128]{2,0,1:T(8,128)(2,1)}) fusion(bf16[16384,2,128]{2,0,1:T(8,128)(2,1)} %all-gather.3.cloned.1.call-done), kind=kLoop, calls=%fused_computation.189 | loop fusion | bytes 16777216 | tf_op jit(solution)/shard_map/split | solution.py:21
  243.8 156.5 %while.15 = (s32[]{:T(128)}, f32[1,2,256]{2,1,0:T(2,128)S(1)}, f32[1,2,256]{2,1,0:T(2,128)S(1)}, f32[1,2,256,128]{3,2,1,0:T(8,128)S(1)}, bf16[64,256,1,128]{3,1,...) while((s32[]{:T(128)}, f32[1,2,256]{2,1,0:T(2,128)S(1)}, ...), condition=%wide.region_5.6_spmd.clone, body=%wide.region_2.5_spmd.clone.sunk | while | flops 68161536 | bytes 2399337 | solution.py:152
  247.4 1.2 fusion.175
  249.9 1.2 fusion.175
  259.7 1.2 fusion.175
  281.7 1.2 fusion.175
  286.6 1.2 fusion.175
  291.5 1.2 fusion.175
  296.4 1.2 fusion.175
  301.3 1.2 fusion.175
  306.1 1.2 fusion.175
  308.6 1.2 fusion.175
  318.4 1.2 fusion.175
  328.2 1.2 fusion.175
  340.4 1.2 fusion.175
  350.2 1.2 fusion.175
  355.1 1.2 fusion.175
  360.0 1.2 fusion.175
  364.9 1.2 fusion.175
  367.3 1.2 fusion.175
  374.6 1.2 fusion.175
  (434 shorter events, 139.5 us)
Async XLA Ops:
  7.2 101.0 %all-gather.5.cloned.1.call-start = ((), (), s32[]{:S(2)}) async-start(), calls=%async_computation.4 | async-start | bytes 11796480 | tf_op jit(solution)/shard_map/all_gather | solution.py:21
  10.5 0.8 copy-start.4
  10.5 1.0 copy-start.9
  10.5 2.5 copy-start.5
  10.5 3.3 copy-start.7
  10.5 4.8 %copy-start = (bf16[128,2048]{1,0:T(8,128)(2,1)S(1)}, bf16[128,2048]{1,0:T(8,128)(2,1)}, u32[]{:S(2)}) copy-start(bf16[128,2048]{1,0:T(8,128)(2,1)} %param.19) | copy-start | bytes 1572868
  10.6 5.0 %copy-start.6 = (f32[2048]{0:T(1024)S(1)}, f32[2048]{0:T(1024)}, u32[]{:S(2)}) copy-start(f32[2048]{0:T(1024)} %param.20) | copy-start | bytes 24580
  10.6 227.5 %all-gather.3.cloned.1.call-start = ((), (), s32[]{:S(2)}) async-start(), calls=%async_computation.3 | async-start | bytes 8519680 | tf_op jit(solution)/shard_map/all_gather | solution.py:21
  144.8 54.1 %copy-start.8 = (f32[128,2]{0,1:T(2,128)S(1)}, f32[128,2]{0,1:T(2,128)}, u32[]{:S(2)}) copy-start(f32[128,2]{0,1:T(2,128)} %param.22) | copy-start | bytes 3076
  144.8 54.8 %copy-start.2 = (f32[256,32]{1,0:T(8,128)S(1)}, f32[256,32]{1,0:T(8,128)}, u32[]{:S(2)}) copy-start(f32[256,32]{1,0:T(8,128)} %get-tuple-element.98) | copy-start | bytes 98308
  144.8 54.8 %copy-start.3 = (f32[256,32]{1,0:T(8,128)S(1)}, f32[256,32]{1,0:T(8,128)}, u32[]{:S(2)}) copy-start(f32[256,32]{1,0:T(8,128)} %get-tuple-element.103) | copy-start | bytes 98308
  144.8 55.4 %copy-start.1 = (bf16[256,2,128]{2,1,0:T(2,128)(2,1)S(1)}, bf16[256,2,128]{2,1,0:T(2,128)(2,1)}, u32[]{:S(2)}) copy-start(bf16[256,2,128]{2,1,0:T(2,128)(2,1)} %param.14) | copy-start | bytes 393220
  144.8 55.6 %copy-start.10 = (f32[128]{0:T(128)S(1)}, f32[128]{0:T(128)}, u32[]{:S(2)}) copy-start(f32[128]{0:T(128)} %param.17) | copy-start | bytes 1540
  192.2 36.0 %all-to-all-start.2 = ((bf16[64,4,1,2048]{3,1,2,0:T(4,128)(2,1)}), bf16[64,4,1,2048]{3,1,2,0:T(4,128)(2,1)}, u32[]{:S(2)}, u32[]{:S(2)}) async-start(bf16[64,4,1,2048]{3,1,2,0:T(4,128)(2,1)} %get-tuple-element.91), calls=%async_computation.2 | async-start | bytes 2097152 | tf_op jit(solution)/shard_map/all_to_all | solution.py:47
Sparse Core Ops, SparseCore 0:
  10.7 97.4 all-gather.4
  111.0 100.6 all-gather.2
where the time goes:
time: 416 us; the launch traced here: 408 us
  matrix products  170 us (41%)
  blocking collectives  111 us (27%)
  local copies, waits for them, and re-layouts  38.2 us (9%)
  waiting for transfers between devices  33.6 us (8%)
  other arithmetic  30.9 us (7%)
  between operations  14.4 us (3%)
  starting transfers between devices  6.7 us (2%)
    dot_general x64, matrix products, merge_block(): jnp.einsum('kgts,skd->kgtd', shifted.astype(jnp.bfloat16), block_values,...  75.9 us
    dot_general x64, matrix products, merge_block(): jnp.einsum('tkgd,skd->kgts', grouped, block_keys, preferred_element_type=...  69.3 us
    all_to_all x1, blocking collectives, on_device(): lax.all_to_all(outgoing, 'ep', split_axis=0, concat_axis=0, tiled=True)  63.6 us
    all_to_all x1, blocking collectives, exchange_in_pieces(): lax.all_to_all(section, axis, split_axis=0, concat_axis=0, tiled=True)  47.4 us
    all_to_all x1, waiting for transfers between devices, exchange_in_pieces(): lax.all_to_all(section, axis, split_axis=0, concat_axis=0, tiled=True)  27.4 us
    unnamed x28, local copies, waits for them, and re-layouts  17.5 us
    dot_general x4, matrix products, on_device(): jnp.einsum('rxf,xfd->rxd', hidden, down_block, preferred_element_type=jnp...  17.2 us
  transfers between devices with their start and end apart: 3, of which 2 were waited for; matrix products, arithmetic and copies ran while one was open for 18% of the time, Pallas kernels for 0%

commit v1 on v0

v1 whole, which is shorter than its diff:
```python
import functools

import jax
import jax.numpy as jnp
from jax import lax
from jax.experimental import pallas as pl
from jax.experimental.pallas import tpu as pltpu
from jax.sharding import PartitionSpec as P

GROUPS = 4
GRID_W = 64
NZ, NY, NC = 8, 4, 2
CAP = 8
LOG2E = 1.4426950408889634

epsilon = 1e-06
rotary_base = 10000.0
floor_value = -1e30

F32 = jnp.float32
BF16 = jnp.bfloat16


def rms(values_f, gain):
    mean = jnp.mean(values_f * values_f, axis=-1, keepdims=True)
    return values_f * lax.rsqrt(mean + epsilon) * gain


def step_kernel(
    n_tp,
    q_ref, k_ref, v_ref, qg_ref, kg_ref, cos_ref, sin_ref,
    rows_ref, mg_ref, ei_ref, rw_ref, gate_ref, up_ref, down_ref,
    att_ref, comb_ref,
    kv, wbuf, out, arr, arr16, total, res, ret, qt, acc, stat, dmat, place,
    loc_sem, ws_sem, wr_sem, zs_sem, zr_sem, ys_sem, yr_sem, cs_sem, cr_sem,
    ds_sem, dr_sem, rs_sem, rr_sem,
):
    me = lax.axis_index("ep")
    t = lax.axis_index("tp")
    z, y, c = me // (NY * NC), (me // NC) % NY, me % NC
    n_ep = NZ * NY * NC

    def ep_of(zz, yy, cc):
        return zz * (NY * NC) + yy * NC + cc

    def ahead(k):
        dz, dy, dc = k % NZ, (k // NZ) % NY, k // (NZ * NY)
        return ep_of((z + dz) % NZ, (y + dy) % NY, (c + dc) % NC)

    def behind(k):
        dz, dy, dc = k % NZ, (k // NZ) % NY, k // (NZ * NY)
        return ep_of((z + NZ - dz) % NZ, (y + NY - dy) % NY, (c + NC - dc) % NC)

    def remote(src, dst, s_sem, r_sem, ep, tp):
        return pltpu.make_async_remote_copy(
            src_ref=src, dst_ref=dst, send_sem=s_sem, recv_sem=r_sem,
            device_id=(ep, tp), device_id_type=pl.DeviceIdType.MESH,
        )

    t_next, t_prev = (t + 1) % n_tp, (t + n_tp - 1) % n_tp

    barrier = pltpu.get_barrier_semaphore()

    @pl.loop(1, n_ep)
    def _(k):
        pl.semaphore_signal(barrier, inc=1, device_id=(ahead(k), t), device_id_type=pl.DeviceIdType.MESH)

    for peer in (t_next, t_prev):
        pl.semaphore_signal(barrier, inc=1, device_id=(me, peer), device_id_type=pl.DeviceIdType.MESH)

    half = wbuf.shape[2] // 2
    srcs = (gate_ref, up_ref, down_ref)

    def w_local(p):
        return pltpu.make_async_copy(srcs[p].at[0], wbuf.at[t, p], loc_sem.at[p])

    for p in range(3):
        w_local(p).start()

    cosine, sine = cos_ref[...], sin_ref[...]

    def turn(x, gain):
        n = rms(x.astype(F32), gain)
        return (n * cosine + pltpu.roll(n, x.shape[-1] // 2, 1) * sine).astype(BF16)

    length, width = k_ref.shape
    kv[c, y, z, 0:length, :] = turn(k_ref[...], kg_ref[...])
    v_t = v_ref[...].astype(F32).T.astype(BF16)
    for j in range(length // width):
        kv[c, y, z, length + j * width : length + (j + 1) * width, :] = v_t[:, j * width : (j + 1) * width]
    for h in range(q_ref.shape[1] // width):
        turned = turn(q_ref[:, h * width : (h + 1) * width], qg_ref[...])
        qt[:, h * length : (h + 1) * length] = turned.astype(F32).T.astype(BF16)

    rows_here, model = rows_ref.shape
    ids = ei_ref[...]
    lanes = lax.broadcasted_iota(jnp.int32, (rows_here, n_ep), 1)
    hot = [(ids[:, k : k + 1] == lanes).astype(F32) for k in range(2)]
    above = (
        lax.broadcasted_iota(jnp.int32, (rows_here, rows_here), 1)
        < lax.broadcasted_iota(jnp.int32, (rows_here, rows_here), 0)
    ).astype(F32).astype(BF16)
    earlier = jnp.dot(above, (hot[0] + hot[1]).astype(BF16), preferred_element_type=F32)
    slots = lax.broadcasted_iota(jnp.int32, (rows_here, n_ep * CAP), 1).astype(F32)
    picks = []
    for k in range(2):
        at = ids[:, k : k + 1].astype(F32) * CAP + jnp.sum(earlier * hot[k], axis=1, keepdims=True)
        pick = (at == slots).astype(F32)
        place[k] = pick.astype(BF16)
        picks.append(pick)
    dmat[...] = (picks[0] + picks[1]).T.astype(BF16)
    arr16[0:rows_here, :] = rms(rows_ref[...].astype(F32), mg_ref[...]).astype(BF16)

    @pl.loop(0, n_ep * CAP // 128)
    def _(i):
        block = jnp.dot(
            dmat[pl.ds(i * 128, 128), :], arr16[0:rows_here, :], preferred_element_type=F32
        )
        out[pl.ds(i * (128 // CAP), 128 // CAP)] = block.reshape(128 // CAP, CAP, model).astype(BF16)

    pl.semaphore_wait(barrier, n_ep - 1 + 2)

    def w_part(first):
        return pl.ds(0, half) if first else pl.ds(half, half)

    def w_copy(d, stage, p):
        to = t_next if d == 0 else t_prev
        part = w_part((d == 0) != (stage == 1))
        sems = (ws_sem.at[d, stage, p], wr_sem.at[d, stage, p])
        if stage < 2:
            return remote(srcs[p].at[0, part], wbuf.at[t, p, part], *sems, me, to)
        held = t_prev if d == 0 else t_next
        return remote(wbuf.at[held, p, part], wbuf.at[held, p, part], *sems, me, to)

    for stage in range(2):
        for p in range(3):
            for d in range(2):
                w_copy(d, stage, p).start()

    def z_copy(dz):
        return remote(
            kv.at[c, y, z], kv.at[c, y, z], zs_sem.at[dz], zr_sem.at[dz], ep_of((z + dz) % NZ, y, c), t
        )

    for dz in (1, 7, 2, 6, 3, 5, 4):
        z_copy(dz).start()

    def d_copy(k):
        return remote(out.at[ahead(k)], arr.at[k], ds_sem.at[k], dr_sem.at[k], ahead(k), t)

    @pl.loop(1, n_ep)
    def _(k):
        d_copy(k).start()

    own = pltpu.make_async_copy(out.at[me], arr.at[0], ds_sem.at[0])
    own.start()

    zh = NZ // 2

    def y_copy(d, stage):
        to = (y + 1) % NY if d == 0 else (y + NY - 1) % NY
        first = (d == 0) != (stage == 1)
        part = pl.ds(0, zh) if first else pl.ds(zh, zh)
        held = y if stage < 2 else ((y + NY - 1) % NY if d == 0 else (y + 1) % NY)
        piece = kv.at[c, held, part]
        return remote(piece, piece, ys_sem.at[d, stage], yr_sem.at[d, stage], ep_of(z, to, c), t)

    def c_copy(dy):
        piece = kv.at[c, (y + dy) % NY]
        return remote(piece, piece, cs_sem.at[dy], cr_sem.at[dy], ep_of(z, y, (c + 1) % NC), t)

    for dz in (1, 7, 2, 6, 3, 5, 4):
        z_copy(dz).wait_recv()
    for stage in range(2):
        for d in range(2):
            y_copy(d, stage).start()
    c_copy(0).start()

    for d in range(2):
        for p in range(3):
            w_copy(d, 0, p).wait_recv()
            w_copy(d, 2, p).start()
    for d in range(2):
        y_copy(d, 0).wait_recv()
        y_copy(d, 2).start()

    @pl.loop(1, n_ep)
    def _(k):
        d_copy(k).wait_recv()

    own.wait()
    arr_chunk = 128

    @pl.loop(0, n_ep * CAP // arr_chunk)
    def _(i):
        block = arr[pl.ds(i * (arr_chunk // CAP), arr_chunk // CAP)].astype(F32)
        arr16[pl.ds(i * arr_chunk, arr_chunk), :] = block.reshape(arr_chunk, model).astype(BF16)

    for p in range(3):
        w_local(p).wait()

    step = 256
    contract = (((1,), (1,)), ((), ()))

    def expert(q, i):
        at = pl.ds(i * step, step)
        x = arr16[at, :]
        g = lax.dot_general(x, wbuf[q, 0], contract, preferred_element_type=F32)
        u = lax.dot_general(x, wbuf[q, 1], contract, preferred_element_type=F32)
        hidden = (g / (1.0 + jnp.exp(-g)) * u).astype(BF16)
        part = jnp.dot(hidden, wbuf[q, 2], preferred_element_type=F32)
        return at, part.astype(BF16).astype(F32)

    chunks = n_ep * CAP // step

    @pl.loop(0, chunks)
    def _(i):
        at, part = expert(t, i)
        total[at, :] = part

    for d, held in ((0, t_prev), (1, t_next)):
        for p in range(3):
            w_copy(d, 1, p).wait_recv()

        @pl.loop(0, chunks)
        def _(i):
            at, part = expert(held, i)
            total[at, :] = total[at, :] + part

    for d in range(2):
        for p in range(3):
            w_copy(d, 2, p).wait_recv()

    def r_copy(k):
        return remote(res.at[k], ret.at[me], rs_sem.at[k], rr_sem.at[k], behind(k), t)

    def r_wait(k):
        return remote(res.at[k], ret.at[ahead(k)], rs_sem.at[k], rr_sem.at[k], behind(k), t)

    last = (t + 2) % n_tp
    per = step // CAP

    @pl.loop(0, chunks)
    def _(i):
        at, part = expert(last, i)
        block = (total[at, :] + part).astype(BF16).astype(F32)
        res[pl.ds(i * per, per)] = block.reshape(per, CAP, model).astype(BF16)

    @pl.loop(1, n_ep)
    def _(k):
        r_copy(k).start()

    mine = pltpu.make_async_copy(res.at[0], ret.at[me], rs_sem.at[0])
    mine.start()

    for d in range(2):
        y_copy(d, 1).wait_recv()
    c_copy(1).start()
    c_copy(3).start()
    for d in range(2):
        y_copy(d, 2).wait_recv()
    c_copy(2).start()
    for dy in range(NY):
        c_copy(dy).wait_recv()

    cols = qt.shape[1]
    factor = width ** (-0.5) * LOG2E
    stat[0:1, :] = jnp.full((1, cols), floor_value, F32)
    stat[1:2, :] = jnp.zeros((1, cols), F32)
    acc[...] = jnp.zeros_like(acc)

    def one_block(b):
        cc, yy, zz = b // (NY * NZ), (b // NZ) % NY, b % NZ
        k_block = kv[cc, yy, zz, 0:length, :]
        v_block = jnp.concatenate(
            [kv[cc, yy, zz, length + j * width : length + (j + 1) * width, :] for j in range(length // width)],
            axis=1,
        )
        s = jnp.dot(k_block, qt[...], preferred_element_type=F32)
        m_b = jnp.max(s, axis=0, keepdims=True)
        p = jnp.exp2((s - m_b) * factor)
        l_b = jnp.sum(p, axis=0, keepdims=True)
        a_b = jnp.dot(v_block, p.astype(BF16), preferred_element_type=F32)
        return m_b, l_b, a_b

    @pl.loop(0, NZ * NY * NC // 2)
    def _(b):
        m_0, l_0, a_0 = one_block(2 * b)
        m_1, l_1, a_1 = one_block(2 * b + 1)
        m_old = stat[0:1, :]
        top = jnp.maximum(jnp.maximum(m_0, m_1), m_old)
        keep = jnp.exp2((m_old - top) * factor)
        n_0 = jnp.exp2((m_0 - top) * factor)
        n_1 = jnp.exp2((m_1 - top) * factor)
        stat[0:1, :] = top
        stat[1:2, :] = stat[1:2, :] * keep + l_0 * n_0 + l_1 * n_1
        acc[...] = acc[...] * keep + a_0 * n_0 + a_1 * n_1

    done = acc[...] / stat[1:2, :]
    for h in range(cols // length):
        att_ref[:, h * width : (h + 1) * width] = done[:, h * length : (h + 1) * length].T.astype(BF16)

    @pl.loop(1, n_ep)
    def _(k):
        r_wait(k).wait_recv()

    mine.wait()

    @pl.loop(0, n_ep * CAP // arr_chunk)
    def _(i):
        block = ret[pl.ds(i * (arr_chunk // CAP), arr_chunk // CAP)].astype(F32)
        arr16[pl.ds(i * arr_chunk, arr_chunk), :] = block.reshape(arr_chunk, model).astype(BF16)

    weights = rw_ref[...]
    wide = 512
    for j in range(model // wide):
        block = arr16[:, j * wide : (j + 1) * wide]
        picked = [jnp.dot(place[k], block, preferred_element_type=F32) * weights[:, k : k + 1] for k in range(2)]
        comb_ref[:, j * wide : (j + 1) * wide] = (picked[0] + picked[1]).astype(BF16)

    for stage in range(3):
        for p in range(3):
            for d in range(2):
                w_copy(d, stage, p).wait_send()
        for d in range(2):
            y_copy(d, stage).wait_send()
    for dz in range(1, NZ):
        z_copy(dz).wait_send()
    for dy in range(NY):
        c_copy(dy).wait_send()

    @pl.loop(1, n_ep)
    def _(k):
        d_copy(k).wait_send()
        r_copy(k).wait_send()


def on_device(
    queries, keys, values, query_gain, key_gain, routed_rows, mixture_gain,
    expert_index, route_weights, expert_gate, expert_up, expert_down,
):
    length, heads, width = queries.shape
    rows_here, model = routed_rows.shape
    n_tp = lax.axis_size("tp")
    n_ep = lax.axis_size("ep")
    slots = n_ep * CAP
    part = expert_gate.shape[1]
    positions = lax.axis_index("ep") * length + jnp.arange(length, dtype=jnp.int32)
    quarter = width // 4
    frequency = rotary_base ** (-jnp.arange(quarter, dtype=F32) / quarter)
    grid_row = (positions // GRID_W).astype(F32)
    grid_col = (positions % GRID_W).astype(F32)
    angles = jnp.concatenate([grid_row[:, None] * frequency, grid_col[:, None] * frequency], axis=-1)
    cosine, sine = jnp.cos(angles), jnp.sin(angles)
    cosine = jnp.concatenate([cosine, cosine], axis=-1)
    sine = jnp.concatenate([-sine, sine], axis=-1)
    vmem = pl.BlockSpec(memory_space=pltpu.VMEM)
    hbm = pl.BlockSpec(memory_space=pl.ANY)
    dma = pltpu.SemaphoreType.DMA
    attended, combined = pl.pallas_call(
        functools.partial(step_kernel, n_tp),
        name="step",
        out_shape=(
            jax.ShapeDtypeStruct((length, heads * width), BF16),
            jax.ShapeDtypeStruct((rows_here, model), BF16),
        ),
        in_specs=[vmem] * 11 + [hbm] * 3,
        out_specs=(vmem, vmem),
        scratch_shapes=[
            pltpu.VMEM((NC, NY, NZ, 2 * length, width), BF16),
            pltpu.VMEM((n_tp, 3, part, model), BF16),
            pltpu.VMEM((n_ep, CAP, model), BF16),
            pltpu.VMEM((n_ep, CAP, model), BF16),
            pltpu.VMEM((slots, model), BF16),
            pltpu.VMEM((slots, model), F32),
            pltpu.VMEM((n_ep, CAP, model), BF16),
            pltpu.VMEM((n_ep, CAP, model), BF16),
            pltpu.VMEM((width, heads * length), BF16),
            pltpu.VMEM((width, heads * length), F32),
            pltpu.VMEM((8, heads * length), F32),
            pltpu.VMEM((slots, rows_here), BF16),
            pltpu.VMEM((2, rows_here, slots), BF16),
            dma((3,)),
            dma((2, 3, 3)),
            dma((2, 3, 3)),
            dma((NZ,)),
            dma((NZ,)),
            dma((2, 3)),
            dma((2, 3)),
            dma((NY,)),
            dma((NY,)),
            dma((n_ep,)),
            dma((n_ep,)),
            dma((n_ep,)),
            dma((n_ep,)),
        ],
        compiler_params=pltpu.CompilerParams(
            collective_id=0, has_side_effects=True, vmem_limit_bytes=60 * 1024 * 1024
        ),
    )(
        queries.reshape(length, heads * width), keys.reshape(length, width), values.reshape(length, width),
        query_gain.reshape(1, width), key_gain.reshape(1, width), cosine, sine,
        routed_rows, mixture_gain.reshape(1, model), expert_index, route_weights,
        expert_gate, expert_up, expert_down,
    )
    return attended.reshape(length, heads, width), combined


def solution(mesh):
    assert dict(mesh.shape) == {"ep": NZ * NY * NC, "tp": 4}
    placed = (
        P("ep", "tp", None),
        P("ep", "tp", None),
        P("ep", "tp", None),
        P(),
        P(),
        P(("ep", "tp"), None),
        P(),
        P(("ep", "tp"), None),
        P(("ep", "tp"), None),
        P("ep", "tp", None),
        P("ep", "tp", None),
        P("ep", "tp", None),
    )
    return jax.shard_map(
        on_device,
        mesh=mesh,
        in_specs=placed,
        out_specs=(P("ep", "tp", None), P(("ep", "tp"), None)),
        check_vma=False,
    )
```

time: 416 us -> 158 us (0.38); the launches traced: 408 us -> 156 us
  matrix products: 170 us -> 0 us
  Pallas kernels: 0 us -> 146 us
  blocking collectives: 111 us -> 0 us
  waiting for transfers between devices: 33.6 us -> 0 us
  local copies, waits for them, and re-layouts: 38.2 us -> 7.01 us
  other arithmetic: 30.9 us -> 2.21 us
  between operations: 14.4 us -> 0.68 us
  starting transfers between devices: 6.7 us -> 0 us
    dot_general x136 -> x0, matrix products: 170 us -> none  [the longest x64 75.9 us: merge_block(): jnp.einsum('kgts,skd->kgtd', shifted.astype(jnp.bfloat16), block_values,...]
    pallas_call x0 -> x1, Pallas kernels: none -> 146 us  [on_device(): pl.pallas_call(functools.partial(step_kernel, n_tp), name='step', out_sha...]
    all_to_all x2 -> x0, blocking collectives: 111 us -> none  [the longest x1 63.6 us: on_device(): lax.all_to_all(outgoing, 'ep', split_axis=0, concat_axis=0, tiled=True)]
    all_to_all x1 -> x0, waiting for transfers between devices: 27.4 us -> none  [exchange_in_pieces(): lax.all_to_all(section, axis, split_axis=0, concat_axis=0, tiled=True)]
    unnamed x28 -> x6, local copies, waits for them, and re-layouts: 17.5 us -> 5.42 us
    reduce_sum x69 -> x0, other arithmetic: 11.4 us -> none  [the longest x64 6.03 us: merge_block(): block_mass = jnp.sum(shifted, axis=-1)]
    split x2 -> x0, local copies, waits for them, and re-layouts: 10.1 us -> none  [the longest x1 5.72 us: side_by_side(): jnp.split(lax.all_gather(both, axis, axis=dim, tiled=True), ends, axis=al...]
    all_to_all x1 -> x0, starting transfers between devices: 6.62 us -> none  [exchange_in_pieces(): lax.all_to_all(section, axis, split_axis=0, concat_axis=0, tiled=True)]
  transfers between devices with their start and end apart: 3 -> 0, of which waited for: 2 -> 0; matrix products, arithmetic and copies ran while one was open for 18% -> 0% of each run, Pallas kernels for 0% -> 0%
where the time goes in v1:
time: 158 us; the launch traced here: 156 us
  Pallas kernels  146 us (92%)
  local copies, waits for them, and re-layouts  7.01 us (4%)
  other arithmetic  2.21 us (1%)
    pallas_call x1, Pallas kernels, on_device(): pl.pallas_call(functools.partial(step_kernel, n_tp), name='step', out_sha...  146 us
    unnamed x6, local copies, waits for them, and re-layouts  5.42 us

profile of v1, /device:TPU:2, one launch (start us, length us, event | category | flops | bytes accessed | tf_op | source)
XLA Modules:
  0.0 155.8 jit_solution(10390019040176566720)
XLA Ops:
  0.6 0.0 copy-start
  0.7 1.4 copy.14.ei_ref
  2.1 1.4 copy.15.rw_ref
  3.5 0.0 copy-done
  3.5 0.7 copy.18
  4.2 0.1 broadcast_multiply_fusion.1
  4.3 0.5 fusion.5
  4.9 0.8 pad_maximum_fusion.2.sin_ref
  5.7 0.8 pad_maximum_fusion.1.cos_ref
  6.4 145.9 %step.1 = (bf16[256,256]{1,0:T(8,128)(2,1)}, bf16[128,2048]{1,0:T(8,128)(2,1)}) custom-call(bf16[256,256]{1,0:T(8,128)(2,1)} %bitcast.9, bf16[256,128]{1,0:T(8,128)(2,1)} %bitcast.11, bf16[256,128]{1,0:T(8,128)(2,1)} %bitcast.12, f32[1,128]{1,0:T(1,128)} %bitcast.14, f32[1,128]{1,0:T(1,128)} %bitcast.15, f32[256,128]{1,0:T(8,128)} %pad_maximum_fusion.1.cos_ref, ...), custom_call_target="tpu_custom_call" | custom-call | tf_op jit(solution)/shard_map/step/pallas_call | solution.py:360
  152.3 1.6 %reshape.71 = bf16[256,2,128]{2,1,0:T(2,128)(2,1)} reshape(bf16[256,256]{1,0:T(8,128)(2,1)} %get-tuple-element.4) | data formatting | bytes 262144 | tf_op jit(solution)/shard_map/reshape | solution.py:406
  153.9 1.9 %copy.20 = bf16[128,2048]{1,0:T(8,128)(2,1)} copy(bf16[128,2048]{1,0:T(8,128)(2,1)} %get-tuple-element.16) | data formatting | bytes 1048576
  (2 shorter events, 0.0 us)
Async XLA Ops:
  0.6 2.9 %copy-start = (bf16[256,2,128]{2,1,0:T(2,128)(2,1)S(1)}, bf16[256,2,128]{2,1,0:T(2,128)(2,1)}, u32[]{:S(2)}) copy-start(bf16[256,2,128]{2,1,0:T(2,128)(2,1)} %param.12) | copy-start | bytes 393220

commit v2 on v1

v2 whole, which is shorter than its diff:
```python
import functools

import jax
import jax.numpy as jnp
import numpy as np
from jax import lax
from jax.experimental import pallas as pl
from jax.experimental.pallas import tpu as pltpu
from jax.sharding import PartitionSpec as P

GROUPS = 4
GRID_W = 64
NZ, NY, NC = 8, 4, 2
CAP = 8
LOG2E = 1.4426950408889634

epsilon = 1e-06
rotary_base = 10000.0
floor_value = -1e30

F32 = jnp.float32
BF16 = jnp.bfloat16


def rms(values_f, gain):
    mean = jnp.mean(values_f * values_f, axis=-1, keepdims=True)
    return values_f * lax.rsqrt(mean + epsilon) * gain


def step_kernel(
    n_tp,
    q_hbm, k_hbm, v_hbm, rows_hbm, row_hbm, col_hbm, gate_ref, up_ref, down_ref,
    qg_ref, kg_ref, mg_ref, ei_ref, rw_ref,
    att_ref, comb_ref,
    q_ref, k_ref, v_ref, rows_ref, row_ref, col_ref,
    kv, wbuf, out, arr, arr16, total, res, ret, qt, acc, stat, dmat, place,
    in_sem, loc_sem, ws_sem, wr_sem, zs_sem, zr_sem, ys_sem, yr_sem, cs_sem, cr_sem,
    ds_sem, dr_sem, rs_sem, rr_sem, go_sem,
):
    me = lax.axis_index("ep")
    t = lax.axis_index("tp")
    z, y, c = me // (NY * NC), (me // NC) % NY, me % NC
    n_ep = NZ * NY * NC
    plane = NZ * NY

    def ep_of(zz, yy, cc):
        return zz * (NY * NC) + yy * NC + cc

    def ahead(k):
        dz, dy, dc = k % NZ, (k // NZ) % NY, k // plane
        return ep_of((z + dz) % NZ, (y + dy) % NY, (c + dc) % NC)

    def behind(k):
        dz, dy, dc = k % NZ, (k // NZ) % NY, k // plane
        return ep_of((z + NZ - dz) % NZ, (y + NY - dy) % NY, (c + NC - dc) % NC)

    def remote(src, dst, s_sem, r_sem, ep, tp):
        return pltpu.make_async_remote_copy(
            src_ref=src, dst_ref=dst, send_sem=s_sem, recv_sem=r_sem,
            device_id=(ep, tp), device_id_type=pl.DeviceIdType.MESH,
        )

    t_next, t_prev = (t + 1) % n_tp, (t + n_tp - 1) % n_tp
    partner = ep_of(z, y, (c + 1) % NC)

    barrier = pltpu.get_barrier_semaphore()
    for peer in (t_next, t_prev):
        pl.semaphore_signal(barrier, inc=1, device_id=(me, peer), device_id_type=pl.DeviceIdType.MESH)

    @pl.loop(1, n_ep)
    def _(k):
        pl.semaphore_signal(barrier, inc=1, device_id=(ahead(k), t), device_id_type=pl.DeviceIdType.MESH)

    half = wbuf.shape[2] // 2
    srcs = (gate_ref, up_ref, down_ref)
    reads = [
        pltpu.make_async_copy(src, dst, in_sem.at[i])
        for i, (src, dst) in enumerate(
            (
                (k_hbm, k_ref), (v_hbm, v_ref), (row_hbm.at[me], row_ref), (col_hbm, col_ref),
                (rows_hbm, rows_ref), (q_hbm, q_ref),
            )
        )
    ]
    for read in reads:
        read.start()

    def w_local(p):
        return pltpu.make_async_copy(srcs[p].at[0], wbuf.at[t, p], loc_sem.at[p])

    pl.semaphore_wait(barrier, n_ep - 1 + 2)

    def w_copy(d, stage, p):
        to = t_next if d == 0 else t_prev
        part = pl.ds(0, half) if (d == 0) != (stage == 1) else pl.ds(half, half)
        sems = (ws_sem.at[d, stage, p], wr_sem.at[d, stage, p])
        if stage < 2:
            return remote(srcs[p].at[0, part], wbuf.at[t, p, part], *sems, me, to)
        held = t_prev if d == 0 else t_next
        return remote(wbuf.at[held, p, part], wbuf.at[held, p, part], *sems, me, to)

    def each_w(stage, act):
        for p in range(3):
            for d in range(2):
                act(w_copy(d, stage, p))

    def start_weights():
        for stage in range(2):
            each_w(stage, lambda copy: copy.start())

    def forward_weights():
        for p in range(3):
            for d in range(2):
                w_copy(d, 0, p).wait_recv()
                w_copy(d, 2, p).start()

    @pl.when(c == 0)
    def _():
        start_weights()

    for p in range(3):
        w_local(p).start()

    for read in reads[:4]:
        read.wait()
    length, width = k_ref.shape
    lines = row_ref.shape[1]
    tables = [
        (row_ref[i][:, None, :] + col_ref[i][None, :, :]).reshape(length, width) for i in range(2)
    ]

    def turn(x, gain):
        n = rms(x.astype(F32), gain)
        return (n * tables[0] + pltpu.roll(n, width // 2, 1) * tables[1]).astype(BF16)

    kv[c, y, z, 0:length, :] = turn(k_ref[...], kg_ref[...])
    v_t = v_ref[...].astype(F32).T.astype(BF16)
    for j in range(length // width):
        kv[c, y, z, length + j * width : length + (j + 1) * width, :] = v_t[:, j * width : (j + 1) * width]

    def z_copy(j):
        step = {1: 1, 7: -1, 2: 2, 6: -2, 3: 1, 5: -1, 4: 2, 0: -2}[j]
        held = z if j in (1, 7, 2, 6) else (z + (NZ - 2 if j in (3, 4) else 2)) % NZ
        piece = kv.at[c, y, held]
        if j == 4:
            piece = kv.at[c, y, held, pl.ds(0, length)]
        if j == 0:
            piece = kv.at[c, y, held, pl.ds(length, length)]
        return remote(piece, piece, zs_sem.at[j], zr_sem.at[j], ep_of((z + step + NZ) % NZ, y, c), t)

    rows_here, model = rows_ref.shape
    pad = jnp.zeros((6, rows_here), F32)
    ids = jnp.concatenate([ei_ref[...].astype(F32), pad], axis=0).T
    lanes = lax.broadcasted_iota(jnp.int32, (rows_here, n_ep), 1).astype(F32)
    hot = [(ids[:, k : k + 1] == lanes).astype(F32) for k in range(2)]
    above = (
        lax.broadcasted_iota(jnp.int32, (rows_here, rows_here), 1)
        < lax.broadcasted_iota(jnp.int32, (rows_here, rows_here), 0)
    ).astype(F32).astype(BF16)
    earlier = jnp.dot(above, (hot[0] + hot[1]).astype(BF16), preferred_element_type=F32)
    slots = lax.broadcasted_iota(jnp.int32, (rows_here, n_ep * CAP), 1).astype(F32)
    picks = []
    for k in range(2):
        at = ids[:, k : k + 1] * CAP + jnp.sum(earlier * hot[k], axis=1, keepdims=True)
        pick = (at == slots).astype(F32)
        place[k] = pick.astype(BF16)
        picks.append(pick)
    dmat[...] = (picks[0] + picks[1]).T.astype(BF16)

    for j in (2, 6, 1, 7):
        z_copy(j).start()

    reads[4].wait()
    arr16[0:rows_here, :] = rms(rows_ref[...].astype(F32), mg_ref[...]).astype(BF16)

    @pl.loop(0, n_ep * CAP // 128)
    def _(i):
        block = jnp.dot(
            dmat[pl.ds(i * 128, 128), :], arr16[0:rows_here, :], preferred_element_type=F32
        )
        out[pl.ds(i * (128 // CAP), 128 // CAP)] = block.reshape(128 // CAP, CAP, model).astype(BF16)

    reads[5].wait()
    for h in range(q_ref.shape[1] // width):
        turned = turn(q_ref[:, h * width : (h + 1) * width], qg_ref[...])
        qt[:, h * length : (h + 1) * length] = turned.astype(F32).T.astype(BF16)

    def d_copy(k):
        return remote(out.at[ahead(k)], arr.at[k], ds_sem.at[k], dr_sem.at[k], ahead(k), t)

    def dispatch(core):
        @pl.loop(0, plane)
        def _(i):
            k = i + plane * ((c + core) % NC)

            @pl.when(k > 0)
            def _():
                d_copy(k).start()

    dispatch(0)
    own = pltpu.make_async_copy(out.at[me], arr.at[0], ds_sem.at[0])
    own.start()
    for j, after in ((2, (3, 4)), (6, (5, 0))):
        z_copy(j).wait_recv()
        for i in after:
            z_copy(i).start()
    dispatch(1)

    zh = NZ // 2

    def y_copy(d, stage):
        to = (y + 1) % NY if d == 0 else (y + NY - 1) % NY
        part = pl.ds(0, zh) if (d == 0) != (stage == 1) else pl.ds(zh, zh)
        held = y if stage < 2 else ((y + NY - 1) % NY if d == 0 else (y + 1) % NY)
        piece = kv.at[c, held, part]
        return remote(piece, piece, ys_sem.at[d, stage], yr_sem.at[d, stage], ep_of(z, to, c), t)

    def c_copy(dy):
        piece = kv.at[c, (y + dy) % NY]
        return remote(piece, piece, cs_sem.at[dy], cr_sem.at[dy], partner, t)

    def start_y():
        for j in (1, 7, 3, 5, 4, 0):
            z_copy(j).wait_recv()
        for stage in range(2):
            for d in range(2):
                y_copy(d, stage).start()
        c_copy(0).start()

    def forward_y():
        for d in range(2):
            y_copy(d, 0).wait_recv()
            y_copy(d, 2).start()

    def near_y():
        for d in range(2):
            y_copy(d, 1).wait_recv()
        c_copy(1).start()
        c_copy(3).start()

    def far_y():
        for d in range(2):
            y_copy(d, 2).wait_recv()
        c_copy(2).start()

    step = 256
    chunks = n_ep * CAP // step
    contract = (((1,), (1,)), ((), ()))

    def expert(q, i):
        at = pl.ds(i * step, step)
        x = arr16[at, :]
        g = lax.dot_general(x, wbuf[q, 0], contract, preferred_element_type=F32)
        u = lax.dot_general(x, wbuf[q, 1], contract, preferred_element_type=F32)
        hidden = (g / (1.0 + jnp.exp(-g)) * u).astype(BF16)
        part = jnp.dot(hidden, wbuf[q, 2], preferred_element_type=F32)
        return at, part.astype(BF16).astype(F32)

    def first_part():
        own.wait()
        for p in range(3):
            w_local(p).wait()
        group = 128 // CAP

        @pl.loop(0, n_ep // group)
        def _(i):
            @pl.loop(0, group)
            def _(j):
                k = i * group + j

                @pl.when(k > 0)
                def _():
                    d_copy(k).wait_recv()

            block = arr[pl.ds(i * group, group)].astype(F32)
            arr16[pl.ds(i * 128, 128), :] = block.reshape(128, model).astype(BF16)

        @pl.loop(0, chunks)
        def _(i):
            at, part = expert(t, i)
            total[at, :] = part

    def add_part(held):
        @pl.loop(0, chunks)
        def _(i):
            at, part = expert(held, i)
            total[at, :] = total[at, :] + part

    def r_copy(k):
        return remote(res.at[k], ret.at[me], rs_sem.at[k], rr_sem.at[k], behind(k), t)

    def r_wait(k):
        return remote(res.at[k], ret.at[ahead(k)], rs_sem.at[k], rr_sem.at[k], behind(k), t)

    mine = pltpu.make_async_copy(res.at[0], ret.at[me], rs_sem.at[0])

    def last_part():
        last = (t + 2) % n_tp
        per = step // CAP

        @pl.loop(0, chunks)
        def _(i):
            at, part = expert(last, i)
            block = (total[at, :] + part).astype(BF16).astype(F32)
            res[pl.ds(i * per, per)] = block.reshape(per, CAP, model).astype(BF16)

        @pl.loop(1, n_ep)
        def _(k):
            r_copy(k).start()

        mine.start()

    cols = qt.shape[1]
    factor = width ** (-0.5) * LOG2E
    stat[0:1, :] = jnp.full((1, cols), floor_value, F32)
    stat[1:2, :] = jnp.zeros((1, cols), F32)
    acc[...] = jnp.zeros_like(acc)

    def one_block(cc, yy, zz):
        k_block = kv[cc, yy, zz, 0:length, :]
        v_block = jnp.concatenate(
            [kv[cc, yy, zz, length + j * width : length + (j + 1) * width, :] for j in range(length // width)],
            axis=1,
        )
        s = jnp.dot(k_block, qt[...], preferred_element_type=F32)
        m_b = jnp.max(s, axis=0, keepdims=True)
        p = jnp.exp2((s - m_b) * factor)
        l_b = jnp.sum(p, axis=0, keepdims=True)
        a_b = jnp.dot(v_block, p.astype(BF16), preferred_element_type=F32)
        return m_b, l_b, a_b

    def attend(dy):
        c_copy(dy).wait_recv()
        yy = (y + dy) % NY

        @pl.loop(0, NZ * NC // 2)
        def _(b):
            cc, zz = b // zh, b % zh
            m_0, l_0, a_0 = one_block(cc, yy, 2 * zz)
            m_1, l_1, a_1 = one_block(cc, yy, 2 * zz + 1)
            m_old = stat[0:1, :]
            top = jnp.maximum(jnp.maximum(m_0, m_1), m_old)
            keep = jnp.exp2((m_old - top) * factor)
            n_0 = jnp.exp2((m_0 - top) * factor)
            n_1 = jnp.exp2((m_1 - top) * factor)
            stat[0:1, :] = top
            stat[1:2, :] = stat[1:2, :] * keep + l_0 * n_0 + l_1 * n_1
            acc[...] = acc[...] * keep + a_0 * n_0 + a_1 * n_1

    @pl.when(c == 0)
    def _():
        forward_weights()
        start_y()
        attend(0)
        first_part()
        each_w(1, lambda copy: copy.wait_recv())
        add_part(t_prev)
        each_w(2, lambda copy: copy.wait_send())
        pl.semaphore_signal(go_sem, inc=1, device_id=(partner, t), device_id_type=pl.DeviceIdType.MESH)
        add_part(t_next)
        each_w(2, lambda copy: copy.wait_recv())
        last_part()
        forward_y()
        near_y()
        attend(1)
        attend(3)

    @pl.when(c == 1)
    def _():
        start_y()
        attend(0)
        pl.semaphore_wait(go_sem, 1)
        start_weights()
        forward_y()
        forward_weights()
        first_part()
        each_w(1, lambda copy: copy.wait_recv())
        add_part(t_prev)
        add_part(t_next)
        near_y()
        attend(1)
        each_w(2, lambda copy: copy.wait_recv())
        last_part()
        attend(3)
        each_w(2, lambda copy: copy.wait_send())

    far_y()
    attend(2)
    done = acc[...] / stat[1:2, :]
    for h in range(cols // length):
        att_ref[:, h * width : (h + 1) * width] = done[:, h * length : (h + 1) * length].T.astype(BF16)

    weights = jnp.concatenate([rw_ref[...], pad], axis=0).T

    @pl.loop(1, n_ep)
    def _(k):
        r_wait(k).wait_recv()

    mine.wait()

    @pl.loop(0, n_ep * CAP // 128)
    def _(i):
        block = ret[pl.ds(i * (128 // CAP), 128 // CAP)].astype(F32)
        arr16[pl.ds(i * 128, 128), :] = block.reshape(128, model).astype(BF16)

    wide = 512
    for j in range(model // wide):
        block = arr16[:, j * wide : (j + 1) * wide]
        picked = [jnp.dot(place[k], block, preferred_element_type=F32) * weights[:, k : k + 1] for k in range(2)]
        comb_ref[:, j * wide : (j + 1) * wide] = (picked[0] + picked[1]).astype(BF16)

    for stage in range(2):
        each_w(stage, lambda copy: copy.wait_send())
    for stage in range(3):
        for d in range(2):
            y_copy(d, stage).wait_send()
    for j in range(NZ):
        z_copy(j).wait_send()
    for dy in range(NY):
        c_copy(dy).wait_send()

    @pl.loop(1, n_ep)
    def _(k):
        d_copy(k).wait_send()
        r_copy(k).wait_send()


def position_tables(count, width):
    quarter = width // 4
    frequency = np.float32(rotary_base) ** (-np.arange(quarter, dtype=np.float32) / np.float32(quarter))
    none = np.zeros((1, quarter))

    def laid(n, first):
        angle = (np.arange(n, dtype=np.float32)[:, None] * frequency).astype(np.float64)
        tables = []
        for value, sign in ((np.cos(angle), 1.0), (np.sin(angle), -1.0)):
            blank = np.broadcast_to(none, value.shape)
            pair = (value, blank) if first else (blank, value)
            tables.append(np.concatenate([sign * pair[0], sign * pair[1], *pair], axis=1))
        return np.stack(tables).astype(np.float32)

    rows = laid(count // GRID_W, True)
    return rows, laid(GRID_W, False)


def on_device(
    queries, keys, values, query_gain, key_gain, routed_rows, mixture_gain,
    expert_index, route_weights, expert_gate, expert_up, expert_down,
):
    length, heads, width = queries.shape
    rows_here, model = routed_rows.shape
    n_tp = lax.axis_size("tp")
    n_ep = lax.axis_size("ep")
    slots = n_ep * CAP
    part = expert_gate.shape[1]
    rows, columns = position_tables(n_ep * length, width)
    rows = jnp.asarray(np.moveaxis(rows.reshape(2, n_ep, length // GRID_W, width), 1, 0))
    vmem = pl.BlockSpec(memory_space=pltpu.VMEM)
    hbm = pl.BlockSpec(memory_space=pl.ANY)
    dma = pltpu.SemaphoreType.DMA
    attended, combined = pl.pallas_call(
        functools.partial(step_kernel, n_tp),
        name="step",
        out_shape=(
            jax.ShapeDtypeStruct((length, heads * width), BF16),
            jax.ShapeDtypeStruct((rows_here, model), BF16),
        ),
        in_specs=[hbm] * 9 + [vmem] * 5,
        out_specs=(vmem, vmem),
        scratch_shapes=[
            pltpu.VMEM((length, heads * width), BF16),
            pltpu.VMEM((length, width), BF16),
            pltpu.VMEM((length, width), BF16),
            pltpu.VMEM((rows_here, model), BF16),
            pltpu.VMEM((2, length // GRID_W, width), F32),
            pltpu.VMEM((2, GRID_W, width), F32),
            pltpu.VMEM((NC, NY, NZ, 2 * length, width), BF16),
            pltpu.VMEM((n_tp, 3, part, model), BF16),
            pltpu.VMEM((n_ep, CAP, model), BF16),
            pltpu.VMEM((n_ep, CAP, model), BF16),
            pltpu.VMEM((slots, model), BF16),
            pltpu.VMEM((slots, model), F32),
            pltpu.VMEM((n_ep, CAP, model), BF16),
            pltpu.VMEM((n_ep, CAP, model), BF16),
            pltpu.VMEM((width, heads * length), BF16),
            pltpu.VMEM((width, heads * length), F32),
            pltpu.VMEM((8, heads * length), F32),
            pltpu.VMEM((slots, rows_here), BF16),
            pltpu.VMEM((2, rows_here, slots), BF16),
            dma((6,)),
            dma((3,)),
            dma((2, 3, 3)),
            dma((2, 3, 3)),
            dma((NZ,)),
            dma((NZ,)),
            dma((2, 3)),
            dma((2, 3)),
            dma((NY,)),
            dma((NY,)),
            dma((n_ep,)),
            dma((n_ep,)),
            dma((n_ep,)),
            dma((n_ep,)),
            pltpu.SemaphoreType.REGULAR,
        ],
        compiler_params=pltpu.CompilerParams(
            collective_id=0, has_side_effects=True, vmem_limit_bytes=60 * 1024 * 1024
        ),
    )(
        queries.reshape(length, heads * width), keys.reshape(length, width), values.reshape(length, width),
        routed_rows, rows, jnp.asarray(columns), expert_gate, expert_up, expert_down,
        query_gain.reshape(1, width), key_gain.reshape(1, width), mixture_gain.reshape(1, model),
        expert_index.T, route_weights.T,
    )
    return attended.reshape(length, heads, width), combined


def solution(mesh):
    assert dict(mesh.shape) == {"ep": NZ * NY * NC, "tp": 4}
    placed = (
        P("ep", "tp", None),
        P("ep", "tp", None),
        P("ep", "tp", None),
        P(),
        P(),
        P(("ep", "tp"), None),
        P(),
        P(("ep", "tp"), None),
        P(("ep", "tp"), None),
        P("ep", "tp", None),
        P("ep", "tp", None),
        P("ep", "tp", None),
    )
    return jax.shard_map(
        on_device,
        mesh=mesh,
        in_specs=placed,
        out_specs=(P("ep", "tp", None), P(("ep", "tp"), None)),
        check_vma=False,
    )
```

time: 158 us -> 147 us (0.930)
  Pallas kernels: 146 us -> 140 us
  other arithmetic: 2.21 us -> 0 us
  local copies, waits for them, and re-layouts: 7.01 us -> 5.05 us
    pallas_call x1, Pallas kernels: 146 us -> 140 us  [on_device(): pl.pallas_call(functools.partial(step_kernel, n_tp), name='step', out_sha...]
    unnamed x6 -> x2, local copies, waits for them, and re-layouts: 5.42 us -> 3.46 us
where the time goes in v2:
time: 147 us; the launch traced here: 146 us
  Pallas kernels  140 us (95%)
  local copies, waits for them, and re-layouts  5.05 us (3%)
    pallas_call x1, Pallas kernels, on_device(): pl.pallas_call(functools.partial(step_kernel, n_tp), name='step', out_sha...  140 us
    unnamed x2, local copies, waits for them, and re-layouts  3.46 us

profile of v2, /device:TPU:2, one launch (start us, length us, event | category | flops | bytes accessed | tf_op | source)
XLA Modules:
  0.0 146.0 jit_solution(13542455614052869341)
XLA Ops:
  0.6 1.6 %copy.18 = bf16[32,8,2,128]{3,1,2,0:T(8,128)(2,1)} copy(bf16[32,8,2,128]{3,2,1,0:T(2,128)(2,1)} %bitcast.12) | data formatting | bytes 262144
  2.2 140.3 %step.1 = (bf16[256,256]{1,0:T(8,128)(2,1)}, bf16[128,2048]{1,0:T(8,128)(2,1)}) custom-call(bf16[256,256]{1,0:T(8,128)(2,1)} %bitcast.11, bf16[256,128]{1,0:T(8,128)(2,1)} %bitcast.13, bf16[256,128]{1,0:T(8,128)(2,1)} %bitcast.14, bf16[128,2048]{1,0:T(8,128)(2,1)} %rows_hbm.1, f32[64,2,4,128]{3,2,1,0:T(4,128)} %constant.4.clone.row_hbm, ...), custom_call_target="tpu_custom_call" | custom-call | tf_op jit(solution)/shard_map/step/pallas_call | solution.py:461
  142.5 1.6 %reshape.31 = bf16[256,2,128]{2,1,0:T(2,128)(2,1)} reshape(bf16[256,256]{1,0:T(8,128)(2,1)} %get-tuple-element.4) | data formatting | bytes 262144 | tf_op jit(solution)/shard_map/reshape | solution.py:515
  144.1 1.9 %copy.20 = bf16[128,2048]{1,0:T(8,128)(2,1)} copy(bf16[128,2048]{1,0:T(8,128)(2,1)} %get-tuple-element.9) | data formatting | bytes 1048576

commit v3 on v2

--- a/solution.py
+++ b/solution.py
@@ -67,9 +67,14 @@
     for peer in (t_next, t_prev):
         pl.semaphore_signal(barrier, inc=1, device_id=(me, peer), device_id_type=pl.DeviceIdType.MESH)
 
-    @pl.loop(1, n_ep)
-    def _(k):
-        pl.semaphore_signal(barrier, inc=1, device_id=(ahead(k), t), device_id_type=pl.DeviceIdType.MESH)
+    z_at = [(z + dz) % NZ for dz in range(NZ)]
+    y_at = [(y + dy) % NY for dy in range(NY)]
+    for dy in (2, 1, 3, 0):
+        for dz in (4, 3, 5, 2, 6, 1, 7, 0):
+            for dc in range(NC):
+                if dz + dy + dc > 0:
+                    peer = ep_of(z_at[dz], y_at[dy], (c + dc) % NC)
+                    pl.semaphore_signal(barrier, inc=1, device_id=(peer, t), device_id_type=pl.DeviceIdType.MESH)
 
     half = wbuf.shape[2] // 2
     srcs = (gate_ref, up_ref, down_ref)
@@ -180,11 +185,6 @@
         )
         out[pl.ds(i * (128 // CAP), 128 // CAP)] = block.reshape(128 // CAP, CAP, model).astype(BF16)
 
-    reads[5].wait()
-    for h in range(q_ref.shape[1] // width):
-        turned = turn(q_ref[:, h * width : (h + 1) * width], qg_ref[...])
-        qt[:, h * length : (h + 1) * length] = turned.astype(F32).T.astype(BF16)
-
     def d_copy(k):
         return remote(out.at[ahead(k)], arr.at[k], ds_sem.at[k], dr_sem.at[k], ahead(k), t)
 
@@ -197,14 +197,19 @@
             def _():
                 d_copy(k).start()
 
-    dispatch(0)
     own = pltpu.make_async_copy(out.at[me], arr.at[0], ds_sem.at[0])
     own.start()
     for j, after in ((2, (3, 4)), (6, (5, 0))):
         z_copy(j).wait_recv()
         for i in after:
             z_copy(i).start()
+    dispatch(0)
     dispatch(1)
+
+    reads[5].wait()
+    for h in range(q_ref.shape[1] // width):
+        turned = turn(q_ref[:, h * width : (h + 1) * width], qg_ref[...])
+        qt[:, h * length : (h + 1) * length] = turned.astype(F32).T.astype(BF16)
 
     zh = NZ // 2
 
@@ -304,9 +309,13 @@
             block = (total[at, :] + part).astype(BF16).astype(F32)
             res[pl.ds(i * per, per)] = block.reshape(per, CAP, model).astype(BF16)
 
-        @pl.loop(1, n_ep)
-        def _(k):
-            r_copy(k).start()
+            @pl.loop(0, per)
+            def _(j):
+                k = i * per + j
+
+                @pl.when(k > 0)
+                def _():
+                    r_copy(k).start()
 
         mine.start()
 
@@ -352,40 +361,42 @@
         forward_weights()
         start_y()
         attend(0)
+        each_w(2, lambda copy: copy.wait_send())
+        pl.semaphore_signal(go_sem, inc=1, device_id=(partner, t), device_id_type=pl.DeviceIdType.MESH)
+        forward_y()
         first_part()
         each_w(1, lambda copy: copy.wait_recv())
         add_part(t_prev)
-        each_w(2, lambda copy: copy.wait_send())
-        pl.semaphore_signal(go_sem, inc=1, device_id=(partner, t), device_id_type=pl.DeviceIdType.MESH)
         add_part(t_next)
         each_w(2, lambda copy: copy.wait_recv())
         last_part()
-        forward_y()
         near_y()
         attend(1)
         attend(3)
+        far_y()
+        attend(2)
 
     @pl.when(c == 1)
     def _():
         start_y()
         attend(0)
+        forward_y()
         pl.semaphore_wait(go_sem, 1)
         start_weights()
-        forward_y()
+        near_y()
         forward_weights()
         first_part()
         each_w(1, lambda copy: copy.wait_recv())
         add_part(t_prev)
         add_part(t_next)
-        near_y()
         attend(1)
+        far_y()
         each_w(2, lambda copy: copy.wait_recv())
         last_part()
         attend(3)
+        attend(2)
         each_w(2, lambda copy: copy.wait_send())
 
-    far_y()
-    attend(2)
     done = acc[...] / stat[1:2, :]
     for h in range(cols // length):
         att_ref[:, h * width : (h + 1) * width] = done[:, h * length : (h + 1) * length].T.astype(BF16)

time: 147 us -> 130 us (0.88)
  Pallas kernels: 140 us -> 123 us
    pallas_call x1, Pallas kernels: 140 us -> 123 us  [on_device(): pl.pallas_call(functools.partial(step_kernel, n_tp), name='step', out_sha...]
where the time goes in v3:
time: 130 us; the launch traced here: 129 us
  Pallas kernels  123 us (95%)
  local copies, waits for them, and re-layouts  5.05 us (4%)
    pallas_call x1, Pallas kernels, on_device(): pl.pallas_call(functools.partial(step_kernel, n_tp), name='step', out_sha...  123 us
    unnamed x2, local copies, waits for them, and re-layouts  3.46 us

profile of v3, /device:TPU:2, one launch (start us, length us, event | category | flops | bytes accessed | tf_op | source)
XLA Modules:
  0.0 128.7 jit_solution(4155168986508886107)
XLA Ops:
  0.6 1.6 %copy.18 = bf16[32,8,2,128]{3,1,2,0:T(8,128)(2,1)} copy(bf16[32,8,2,128]{3,2,1,0:T(2,128)(2,1)} %bitcast.12) | data formatting | bytes 262144
  2.2 123.0 %step.1 = (bf16[256,256]{1,0:T(8,128)(2,1)}, bf16[128,2048]{1,0:T(8,128)(2,1)}) custom-call(bf16[256,256]{1,0:T(8,128)(2,1)} %bitcast.11, bf16[256,128]{1,0:T(8,128)(2,1)} %bitcast.13, bf16[256,128]{1,0:T(8,128)(2,1)} %bitcast.14, bf16[128,2048]{1,0:T(8,128)(2,1)} %rows_hbm.1, f32[64,2,4,128]{3,2,1,0:T(4,128)} %constant.4.clone.row_hbm, ...), custom_call_target="tpu_custom_call" | custom-call | tf_op jit(solution)/shard_map/step/pallas_call | solution.py:472
  125.2 1.6 %reshape.31 = bf16[256,2,128]{2,1,0:T(2,128)(2,1)} reshape(bf16[256,256]{1,0:T(8,128)(2,1)} %get-tuple-element.4) | data formatting | bytes 262144 | tf_op jit(solution)/shard_map/reshape | solution.py:526
  126.8 1.9 %copy.20 = bf16[128,2048]{1,0:T(8,128)(2,1)} copy(bf16[128,2048]{1,0:T(8,128)(2,1)} %get-tuple-element.9) | data formatting | bytes 1048576

commit v4 on v3

--- a/solution.py
+++ b/solution.py
@@ -31,10 +31,10 @@
     n_tp,
     q_hbm, k_hbm, v_hbm, rows_hbm, row_hbm, col_hbm, gate_ref, up_ref, down_ref,
     qg_ref, kg_ref, mg_ref, ei_ref, rw_ref,
-    att_ref, comb_ref,
-    q_ref, k_ref, v_ref, rows_ref, row_ref, col_ref,
-    kv, wbuf, out, arr, arr16, total, res, ret, qt, acc, stat, dmat, place,
-    in_sem, loc_sem, ws_sem, wr_sem, zs_sem, zr_sem, ys_sem, yr_sem, cs_sem, cr_sem,
+    att_out, comb_out,
+    att_ref, comb_ref, q_ref, k_ref, v_ref, rows_ref, row_ref, col_ref,
+    kv, wbuf, out, arr, arr16, total, hid, res, ret, qt, acc, stat, dmat, place,
+    in_sem, out_sem, loc_sem, own_sem, ws_sem, wr_sem, zs_sem, zr_sem, ys_sem, yr_sem, cs_sem, cr_sem,
     ds_sem, dr_sem, rs_sem, rr_sem, go_sem,
 ):
     me = lax.axis_index("ep")
@@ -46,13 +46,8 @@
     def ep_of(zz, yy, cc):
         return zz * (NY * NC) + yy * NC + cc
 
-    def ahead(k):
-        dz, dy, dc = k % NZ, (k // NZ) % NY, k // plane
-        return ep_of((z + dz) % NZ, (y + dy) % NY, (c + dc) % NC)
-
-    def behind(k):
-        dz, dy, dc = k % NZ, (k // NZ) % NY, k // plane
-        return ep_of((z + NZ - dz) % NZ, (y + NY - dy) % NY, (c + NC - dc) % NC)
+    def line(ep):
+        return (ep % NC) * plane + ep // NC
 
     def remote(src, dst, s_sem, r_sem, ep, tp):
         return pltpu.make_async_remote_copy(
@@ -60,8 +55,14 @@
             device_id=(ep, tp), device_id_type=pl.DeviceIdType.MESH,
         )
 
+    def sent(ref, sem):
+        remote(ref, ref, sem, sem, partner, t).wait_send()
+
+    def landed(ref, sem):
+        remote(ref, ref, sem, sem, partner, t).wait_recv()
+
+    partner = ep_of(z, y, (c + 1) % NC)
     t_next, t_prev = (t + 1) % n_tp, (t + n_tp - 1) % n_tp
-    partner = ep_of(z, y, (c + 1) % NC)
 
     barrier = pltpu.get_barrier_semaphore()
     for peer in (t_next, t_prev):
@@ -98,7 +99,10 @@
     def w_copy(d, stage, p):
         to = t_next if d == 0 else t_prev
         part = pl.ds(0, half) if (d == 0) != (stage == 1) else pl.ds(half, half)
-        sems = (ws_sem.at[d, stage, p], wr_sem.at[d, stage, p])
+        sems = (
+            ws_sem.at[p if stage == 2 else 3],
+            wr_sem.at[(3 * d + p, 6, 7 + p // 2)[stage]],
+        )
         if stage < 2:
             return remote(srcs[p].at[0, part], wbuf.at[t, p, part], *sems, me, to)
         held = t_prev if d == 0 else t_next
@@ -144,14 +148,14 @@
         kv[c, y, z, length + j * width : length + (j + 1) * width, :] = v_t[:, j * width : (j + 1) * width]
 
     def z_copy(j):
-        step = {1: 1, 7: -1, 2: 2, 6: -2, 3: 1, 5: -1, 4: 2, 0: -2}[j]
-        held = z if j in (1, 7, 2, 6) else (z + (NZ - 2 if j in (3, 4) else 2)) % NZ
+        step, back = {1: (1, 0), 2: (2, 0), 3: (1, 2), 4: (2, 2), 7: (-1, 0), 6: (-2, 0), 5: (-1, -2), 0: (-2, -2)}[j]
+        held = (z - back + NZ) % NZ
         piece = kv.at[c, y, held]
         if j == 4:
             piece = kv.at[c, y, held, pl.ds(0, length)]
         if j == 0:
             piece = kv.at[c, y, held, pl.ds(length, length)]
-        return remote(piece, piece, zs_sem.at[j], zr_sem.at[j], ep_of((z + step + NZ) % NZ, y, c), t)
+        return remote(piece, piece, zs_sem.at[0], zr_sem.at[{2: 1, 6: 2}.get(j, 0)], ep_of((z + step + NZ) % NZ, y, c), t)
 
     rows_here, model = rows_ref.shape
     pad = jnp.zeros((6, rows_here), F32)
@@ -166,7 +170,9 @@
     slots = lax.broadcasted_iota(jnp.int32, (rows_here, n_ep * CAP), 1).astype(F32)
     picks = []
     for k in range(2):
-        at = ids[:, k : k + 1] * CAP + jnp.sum(earlier * hot[k], axis=1, keepdims=True)
+        upper = jnp.floor(ids[:, k : k + 1] * (1.0 / NC))
+        row = (ids[:, k : k + 1] - upper * NC) * plane + upper
+        at = row * CAP + jnp.sum(earlier * hot[k], axis=1, keepdims=True)
         pick = (at == slots).astype(F32)
         place[k] = pick.astype(BF16)
         picks.append(pick)
@@ -185,19 +191,28 @@
         )
         out[pl.ds(i * (128 // CAP), 128 // CAP)] = block.reshape(128 // CAP, CAP, model).astype(BF16)
 
-    def d_copy(k):
-        return remote(out.at[ahead(k)], arr.at[k], ds_sem.at[k], dr_sem.at[k], ahead(k), t)
+    def alternate(i):
+        side = 1 - 2 * (i % 2)
+        return (NZ // 2 + side * ((i + 1) // 2) + NZ) % NZ
 
     def dispatch(core):
-        @pl.loop(0, plane)
-        def _(i):
-            k = i + plane * ((c + core) % NC)
-
-            @pl.when(k > 0)
-            def _():
-                d_copy(k).start()
-
-    own = pltpu.make_async_copy(out.at[me], arr.at[0], ds_sem.at[0])
+        dc = (c + core) % NC
+        for dy in range(NY):
+
+            @pl.loop(0, NZ)
+            def _(i):
+                dz = alternate(i)
+                row = (z + dz) % NZ * NY + y_at[dy]
+                k = dc * plane + dy * NZ + dz
+                copy = remote(
+                    out.at[core * plane + row], arr.at[k], ds_sem.at[0], dr_sem.at[2 * dc + dy // 2], row * NC + core, t
+                )
+                if dy > 0:
+                    copy.start()
+                else:
+                    pl.when(k > 0)(copy.start)
+
+    own = pltpu.make_async_copy(out.at[line(me)], arr.at[0], own_sem.at[0])
     own.start()
     for j, after in ((2, (3, 4)), (6, (5, 0))):
         z_copy(j).wait_recv()
@@ -207,8 +222,9 @@
     dispatch(1)
 
     reads[5].wait()
-    for h in range(q_ref.shape[1] // width):
-        turned = turn(q_ref[:, h * width : (h + 1) * width], qg_ref[...])
+    q_f = q_ref[...].astype(F32)
+    for h in range(q_ref.shape[1]):
+        turned = turn(q_f[:, h, :], qg_ref[...])
         qt[:, h * length : (h + 1) * length] = turned.astype(F32).T.astype(BF16)
 
     zh = NZ // 2
@@ -218,15 +234,14 @@
         part = pl.ds(0, zh) if (d == 0) != (stage == 1) else pl.ds(zh, zh)
         held = y if stage < 2 else ((y + NY - 1) % NY if d == 0 else (y + 1) % NY)
         piece = kv.at[c, held, part]
-        return remote(piece, piece, ys_sem.at[d, stage], yr_sem.at[d, stage], ep_of(z, to, c), t)
+        return remote(piece, piece, ys_sem.at[0], yr_sem.at[d if stage == 0 else stage + 1], ep_of(z, to, c), t)
 
     def c_copy(dy):
         piece = kv.at[c, (y + dy) % NY]
-        return remote(piece, piece, cs_sem.at[dy], cr_sem.at[dy], partner, t)
+        return remote(piece, piece, cs_sem.at[0], cr_sem.at[dy], partner, t)
 
     def start_y():
-        for j in (1, 7, 3, 5, 4, 0):
-            z_copy(j).wait_recv()
+        landed(kv.at[c, y, pl.ds(0, 5)], zr_sem.at[0])
         for stage in range(2):
             for d in range(2):
                 y_copy(d, stage).start()
@@ -238,27 +253,26 @@
             y_copy(d, 2).start()
 
     def near_y():
-        for d in range(2):
-            y_copy(d, 1).wait_recv()
+        landed(kv.at[c, 0], yr_sem.at[2])
         c_copy(1).start()
         c_copy(3).start()
 
     def far_y():
-        for d in range(2):
-            y_copy(d, 2).wait_recv()
+        landed(kv.at[c, 0], yr_sem.at[3])
         c_copy(2).start()
 
     step = 256
     chunks = n_ep * CAP // step
     contract = (((1,), (1,)), ((), ()))
 
+    def hidden_of(x, q):
+        g = lax.dot_general(x, wbuf[q, 0], contract, preferred_element_type=F32)
+        u = lax.dot_general(x, wbuf[q, 1], contract, preferred_element_type=F32)
+        return (g / (1.0 + jnp.exp(-g)) * u).astype(BF16)
+
     def expert(q, i):
         at = pl.ds(i * step, step)
-        x = arr16[at, :]
-        g = lax.dot_general(x, wbuf[q, 0], contract, preferred_element_type=F32)
-        u = lax.dot_general(x, wbuf[q, 1], contract, preferred_element_type=F32)
-        hidden = (g / (1.0 + jnp.exp(-g)) * u).astype(BF16)
-        part = jnp.dot(hidden, wbuf[q, 2], preferred_element_type=F32)
+        part = jnp.dot(hidden_of(arr16[at, :], q), wbuf[q, 2], preferred_element_type=F32)
         return at, part.astype(BF16).astype(F32)
 
     def first_part():
@@ -267,18 +281,11 @@
             w_local(p).wait()
         group = 128 // CAP
 
-        @pl.loop(0, n_ep // group)
-        def _(i):
-            @pl.loop(0, group)
-            def _(j):
-                k = i * group + j
-
-                @pl.when(k > 0)
-                def _():
-                    d_copy(k).wait_recv()
-
-            block = arr[pl.ds(i * group, group)].astype(F32)
-            arr16[pl.ds(i * 128, 128), :] = block.reshape(128, model).astype(BF16)
+        for i in range(n_ep // group):
+            low = max(i * group, 1)
+            landed(arr.at[pl.ds(low, (i + 1) * group - low)], dr_sem.at[i])
+            block = arr[i * group : (i + 1) * group].astype(F32)
+            arr16[i * 128 : (i + 1) * 128, :] = block.reshape(128, model).astype(BF16)
 
         @pl.loop(0, chunks)
         def _(i):
@@ -291,31 +298,43 @@
             at, part = expert(held, i)
             total[at, :] = total[at, :] + part
 
-    def r_copy(k):
-        return remote(res.at[k], ret.at[me], rs_sem.at[k], rr_sem.at[k], behind(k), t)
-
-    def r_wait(k):
-        return remote(res.at[k], ret.at[ahead(k)], rs_sem.at[k], rr_sem.at[k], behind(k), t)
-
-    mine = pltpu.make_async_copy(res.at[0], ret.at[me], rs_sem.at[0])
+    mine = pltpu.make_async_copy(res.at[0], ret.at[line(me)], own_sem.at[1])
 
     def last_part():
         last = (t + 2) % n_tp
         per = step // CAP
+        landed(wbuf.at[0, pl.ds(0, 2)], wr_sem.at[7])
 
         @pl.loop(0, chunks)
         def _(i):
-            at, part = expert(last, i)
+            at = pl.ds(i * step, step)
+            hid[at, :] = hidden_of(arr16[at, :], last)
+
+        landed(wbuf.at[0, 2], wr_sem.at[8])
+
+        @pl.loop(0, chunks)
+        def _(i):
+            at = pl.ds(i * step, step)
+            part = jnp.dot(hid[at, :], wbuf[last, 2], preferred_element_type=F32).astype(BF16).astype(F32)
             block = (total[at, :] + part).astype(BF16).astype(F32)
             res[pl.ds(i * per, per)] = block.reshape(per, CAP, model).astype(BF16)
 
-            @pl.loop(0, per)
-            def _(j):
-                k = i * per + j
-
-                @pl.when(k > 0)
-                def _():
-                    r_copy(k).start()
+            core = (c + i) % NC
+
+            for dy in range(NY):
+
+                @pl.loop(0, NZ)
+                def _(j):
+                    dz = alternate(j)
+                    row = (z + NZ - dz) % NZ * NY + y_at[(NY - dy) % NY]
+                    k = i * plane + dy * NZ + dz
+                    copy = remote(
+                        res.at[k], ret.at[line(me)], rs_sem.at[0], rr_sem.at[i], row * NC + core, t
+                    )
+                    if dy > 0:
+                        copy.start()
+                    else:
+                        pl.when(k > 0)(copy.start)
 
         mine.start()
 
@@ -338,13 +357,12 @@
         a_b = jnp.dot(v_block, p.astype(BF16), preferred_element_type=F32)
         return m_b, l_b, a_b
 
-    def attend(dy):
-        c_copy(dy).wait_recv()
+    def attend(dy, core):
         yy = (y + dy) % NY
 
-        @pl.loop(0, NZ * NC // 2)
-        def _(b):
-            cc, zz = b // zh, b % zh
+        @pl.loop(0, zh)
+        def _(zz):
+            cc = (c + core) % NC
             m_0, l_0, a_0 = one_block(cc, yy, 2 * zz)
             m_1, l_1, a_1 = one_block(cc, yy, 2 * zz + 1)
             m_old = stat[0:1, :]
@@ -360,80 +378,106 @@
     def _():
         forward_weights()
         start_y()
-        attend(0)
-        each_w(2, lambda copy: copy.wait_send())
+        attend(0, 0)
+        c_copy(0).wait_recv()
+        attend(0, 1)
+        for p in range(2):
+            sent(wbuf.at[0, p], ws_sem.at[p])
         pl.semaphore_signal(go_sem, inc=1, device_id=(partner, t), device_id_type=pl.DeviceIdType.MESH)
         forward_y()
         first_part()
-        each_w(1, lambda copy: copy.wait_recv())
+        landed(wbuf.at[0], wr_sem.at[6])
         add_part(t_prev)
         add_part(t_next)
-        each_w(2, lambda copy: copy.wait_recv())
         last_part()
         near_y()
-        attend(1)
-        attend(3)
+        for dy in (1, 3):
+            attend(dy, 0)
+        for dy in (1, 3):
+            c_copy(dy).wait_recv()
+            attend(dy, 1)
         far_y()
-        attend(2)
+        attend(2, 0)
+        c_copy(2).wait_recv()
+        attend(2, 1)
 
     @pl.when(c == 1)
     def _():
         start_y()
-        attend(0)
+        attend(0, 0)
+        c_copy(0).wait_recv()
+        attend(0, 1)
         forward_y()
         pl.semaphore_wait(go_sem, 1)
         start_weights()
         near_y()
+        attend(1, 0)
         forward_weights()
+        attend(3, 0)
         first_part()
-        each_w(1, lambda copy: copy.wait_recv())
+        landed(wbuf.at[0], wr_sem.at[6])
         add_part(t_prev)
         add_part(t_next)
-        attend(1)
         far_y()
-        each_w(2, lambda copy: copy.wait_recv())
+        attend(2, 0)
         last_part()
-        attend(3)
-        attend(2)
-        each_w(2, lambda copy: copy.wait_send())
+        for dy in (1, 3, 2):
+            c_copy(dy).wait_recv()
+            attend(dy, 1)
+        for p in range(2):
+            sent(wbuf.at[0, p], ws_sem.at[p])
 
     done = acc[...] / stat[1:2, :]
-    for h in range(cols // length):
-        att_ref[:, h * width : (h + 1) * width] = done[:, h * length : (h + 1) * length].T.astype(BF16)
+    heads = [done[:, h * length : (h + 1) * length].T for h in range(cols // length)]
+    att_ref[...] = jnp.stack(heads, axis=1).astype(BF16)
+    writes = [pltpu.make_async_copy(att_ref, att_out, out_sem.at[4])]
+    writes[0].start()
+
+    sent(wbuf.at[pl.ds(0, 2)], ws_sem.at[3])
+    sent(wbuf.at[0, 2], ws_sem.at[2])
+    sent(kv.at[c, y, pl.ds(0, NZ - 1)], zs_sem.at[0])
+    sent(kv.at[c, pl.ds(0, NY - 1)], ys_sem.at[0])
+    sent(kv.at[c], cs_sem.at[0])
+    sent(out.at[pl.ds(0, n_ep - 1)], ds_sem.at[0])
 
     weights = jnp.concatenate([rw_ref[...], pad], axis=0).T
-
-    @pl.loop(1, n_ep)
-    def _(k):
-        r_wait(k).wait_recv()
-
-    mine.wait()
-
-    @pl.loop(0, n_ep * CAP // 128)
-    def _(i):
-        block = ret[pl.ds(i * (128 // CAP), 128 // CAP)].astype(F32)
-        arr16[pl.ds(i * 128, 128), :] = block.reshape(128, model).astype(BF16)
-
     wide = 512
-    for j in range(model // wide):
-        block = arr16[:, j * wide : (j + 1) * wide]
-        picked = [jnp.dot(place[k], block, preferred_element_type=F32) * weights[:, k : k + 1] for k in range(2)]
-        comb_ref[:, j * wide : (j + 1) * wide] = (picked[0] + picked[1]).astype(BF16)
-
-    for stage in range(2):
-        each_w(stage, lambda copy: copy.wait_send())
-    for stage in range(3):
-        for d in range(2):
-            y_copy(d, stage).wait_send()
-    for j in range(NZ):
-        z_copy(j).wait_send()
-    for dy in range(NY):
-        c_copy(dy).wait_send()
-
-    @pl.loop(1, n_ep)
-    def _(k):
-        d_copy(k).wait_send()
-        r_copy(k).wait_send()
+
+    def take(core):
+        @pl.when(c == core)
+        def _():
+            landed(ret.at[pl.ds(core * plane, plane - 1)], rr_sem.at[0])
+            mine.wait()
+
+        @pl.when(c != core)
+        def _():
+            landed(ret.at[pl.ds(core * plane, plane)], rr_sem.at[1])
+
+        lines = plane * CAP
+        for i in range(lines // 128):
+            first = core * plane + i * (128 // CAP)
+            block = ret[first : first + 128 // CAP].astype(F32)
+            arr16[first * CAP : first * CAP + 128, :] = block.reshape(128, model).astype(BF16)
+        for j in range(model // wide):
+            block = arr16[core * lines : (core + 1) * lines, j * wide : (j + 1) * wide]
+            picked = [
+                jnp.dot(place[k, :, core * lines : (core + 1) * lines], block, preferred_element_type=F32)
+                * weights[:, k : k + 1]
+                for k in range(2)
+            ]
+            yield pl.ds(j * wide, wide), picked[0] + picked[1]
+
+    for at, value in take(0):
+        total[0:rows_here, at] = value
+
+    sent(res.at[pl.ds(0, n_ep - 1)], rs_sem.at[0])
+
+    for i, (at, value) in enumerate(take(1)):
+        comb_ref[:, at] = (total[0:rows_here, at] + value).astype(BF16)
+        writes.append(pltpu.make_async_copy(comb_ref.at[:, at], comb_out.at[:, at], out_sem.at[i]))
+        writes[-1].start()
+    for write in writes:
+        write.wait()
 
 
 def position_tables(count, width):
@@ -473,13 +517,15 @@
         functools.partial(step_kernel, n_tp),
         name="step",
         out_shape=(
-            jax.ShapeDtypeStruct((length, heads * width), BF16),
+            jax.ShapeDtypeStruct((length, heads, width), BF16),
             jax.ShapeDtypeStruct((rows_here, model), BF16),
         ),
         in_specs=[hbm] * 9 + [vmem] * 5,
-        out_specs=(vmem, vmem),
+        out_specs=(hbm, hbm),
         scratch_shapes=[
-            pltpu.VMEM((length, heads * width), BF16),
+            pltpu.VMEM((length, heads, width), BF16),
+            pltpu.VMEM((rows_here, model), BF16),
+            pltpu.VMEM((length, heads, width), BF16),
             pltpu.VMEM((length, width), BF16),
             pltpu.VMEM((length, width), BF16),
             pltpu.VMEM((rows_here, model), BF16),
@@ -491,6 +537,7 @@
             pltpu.VMEM((n_ep, CAP, model), BF16),
             pltpu.VMEM((slots, model), BF16),
             pltpu.VMEM((slots, model), F32),
+            pltpu.VMEM((slots, part), BF16),
             pltpu.VMEM((n_ep, CAP, model), BF16),
             pltpu.VMEM((n_ep, CAP, model), BF16),
             pltpu.VMEM((width, heads * length), BF16),
@@ -499,31 +546,33 @@
             pltpu.VMEM((slots, rows_here), BF16),
             pltpu.VMEM((2, rows_here, slots), BF16),
             dma((6,)),
+            dma((5,)),
             dma((3,)),
-            dma((2, 3, 3)),
-            dma((2, 3, 3)),
-            dma((NZ,)),
-            dma((NZ,)),
-            dma((2, 3)),
-            dma((2, 3)),
+            dma((2,)),
+            dma((4,)),
+            dma((9,)),
+            dma((1,)),
+            dma((3,)),
+            dma((1,)),
+            dma((4,)),
+            dma((1,)),
             dma((NY,)),
-            dma((NY,)),
-            dma((n_ep,)),
-            dma((n_ep,)),
-            dma((n_ep,)),
-            dma((n_ep,)),
+            dma((1,)),
+            dma((4,)),
+            dma((1,)),
+            dma((2,)),
             pltpu.SemaphoreType.REGULAR,
         ],
         compiler_params=pltpu.CompilerParams(
             collective_id=0, has_side_effects=True, vmem_limit_bytes=60 * 1024 * 1024
         ),
     )(
-        queries.reshape(length, heads * width), keys.reshape(length, width), values.reshape(length, width),
+        queries, keys.reshape(length, width), values.reshape(length, width),
         routed_rows, rows, jnp.asarray(columns), expert_gate, expert_up, expert_down,
         query_gain.reshape(1, width), key_gain.reshape(1, width), mixture_gain.reshape(1, model),
         expert_index.T, route_weights.T,
     )
-    return attended.reshape(length, heads, width), combined
+    return attended, combined
 
 
 def solution(mesh):

time: 130 us -> 124 us (0.954); the launches traced: 129 us -> 124 us
  Pallas kernels: 123 us -> 120 us
  local copies, waits for them, and re-layouts: 5.05 us -> 3.53 us
    pallas_call x1, Pallas kernels: 123 us -> 120 us  [on_device(): pl.pallas_call(functools.partial(step_kernel, n_tp), name='step', out_sha...]
    reshape x1 -> x0, local copies, waits for them, and re-layouts: 1.6 us -> none  [on_device(): return (attended.reshape(length, heads, width), combined)]
where the time goes in v4:
time: 124 us
  Pallas kernels  120 us (97%)
  local copies, waits for them, and re-layouts  3.53 us (3%)
    pallas_call x1, Pallas kernels, on_device(): pl.pallas_call(functools.partial(step_kernel, n_tp), name='step', out_sha...  120 us
    unnamed x2, local copies, waits for them, and re-layouts  3.53 us

profile of v4, /device:TPU:2, one launch (start us, length us, event | category | flops | bytes accessed | tf_op | source)
XLA Modules:
  0.0 124.3 jit_solution(14767802238046877109)
XLA Ops:
  0.6 120.1 %step.1 = (bf16[256,2,128]{2,1,0:T(2,128)(2,1)}, bf16[128,2048]{1,0:T(8,128)(2,1)}) custom-call(bf16[256,2,128]{2,1,0:T(2,128)(2,1)} %q_hbm.1, bf16[256,128]{1,0:T(8,128)(2,1)} %bitcast.7, bf16[256,128]{1,0:T(8,128)(2,1)} %bitcast.8, bf16[128,2048]{1,0:T(8,128)(2,1)} %rows_hbm.1, f32[64,2,4,128]{3,2,1,0:T(4,128)} %constant.4.clone.row_hbm, ...), custom_call_target="tpu_custom_call" | custom-call | tf_op jit(solution)/shard_map/step/pallas_call | solution.py:516
  120.7 1.7 %copy.18 = bf16[256,2,128]{2,1,0:T(2,128)(2,1)} copy(bf16[256,2,128]{2,1,0:T(2,128)(2,1)} %get-tuple-element.4) | data formatting | bytes 262144
  122.4 1.9 %copy.19 = bf16[128,2048]{1,0:T(8,128)(2,1)} copy(bf16[128,2048]{1,0:T(8,128)(2,1)} %get-tuple-element.5) | data formatting | bytes 1048576

commit v5 on v4

--- a/solution.py
+++ b/solution.py
@@ -148,14 +148,14 @@
         kv[c, y, z, length + j * width : length + (j + 1) * width, :] = v_t[:, j * width : (j + 1) * width]
 
     def z_copy(j):
-        step, back = {1: (1, 0), 2: (2, 0), 3: (1, 2), 4: (2, 2), 7: (-1, 0), 6: (-2, 0), 5: (-1, -2), 0: (-2, -2)}[j]
+        step, back = {1: (1, 0), 2: (1, 1), 3: (1, 2), 4: (1, 3), 7: (-1, 0), 6: (-1, -1), 5: (-1, -2), 0: (-1, -3)}[j]
         held = (z - back + NZ) % NZ
         piece = kv.at[c, y, held]
         if j == 4:
             piece = kv.at[c, y, held, pl.ds(0, length)]
         if j == 0:
             piece = kv.at[c, y, held, pl.ds(length, length)]
-        return remote(piece, piece, zs_sem.at[0], zr_sem.at[{2: 1, 6: 2}.get(j, 0)], ep_of((z + step + NZ) % NZ, y, c), t)
+        return remote(piece, piece, zs_sem.at[0], zr_sem.at[{1: 1, 7: 2, 2: 3, 6: 4, 3: 5, 5: 6}.get(j, 0)], ep_of((z + step + NZ) % NZ, y, c), t)
 
     rows_here, model = rows_ref.shape
     pad = jnp.zeros((6, rows_here), F32)
@@ -178,7 +178,7 @@
         picks.append(pick)
     dmat[...] = (picks[0] + picks[1]).T.astype(BF16)
 
-    for j in (2, 6, 1, 7):
+    for j in (1, 7):
         z_copy(j).start()
 
     reads[4].wait()
@@ -195,29 +195,42 @@
         side = 1 - 2 * (i % 2)
         return (NZ // 2 + side * ((i + 1) // 2) + NZ) % NZ
 
-    def dispatch(core):
+    def beyond(i):
+        return alternate(i) * (1 - i // 5)
+
+    def send_row(core, dz, dy):
         dc = (c + core) % NC
-        for dy in range(NY):
-
-            @pl.loop(0, NZ)
-            def _(i):
-                dz = alternate(i)
-                row = (z + dz) % NZ * NY + y_at[dy]
-                k = dc * plane + dy * NZ + dz
-                copy = remote(
-                    out.at[core * plane + row], arr.at[k], ds_sem.at[0], dr_sem.at[2 * dc + dy // 2], row * NC + core, t
-                )
-                if dy > 0:
-                    copy.start()
-                else:
-                    pl.when(k > 0)(copy.start)
+        row = (z + dz) % NZ * NY + y_at[dy]
+        k = dc * plane + dy * NZ + dz
+        copy = remote(
+            out.at[core * plane + row], arr.at[k], ds_sem.at[0], dr_sem.at[2 * dc + dy // 2], row * NC + core, t
+        )
+        if dy > 0:
+            copy.start()
+        else:
+            pl.when(k > 0)(copy.start)
 
     own = pltpu.make_async_copy(out.at[line(me)], arr.at[0], own_sem.at[0])
     own.start()
-    for j, after in ((2, (3, 4)), (6, (5, 0))):
-        z_copy(j).wait_recv()
-        for i in after:
-            z_copy(i).start()
+    fill = [(core, dy) for core in range(NC) for dy in range(NY)]
+    hops = ((1, 7), (2, 6), (3, 5), (4, 0))
+    for i in range(4):
+        if i > 0:
+            for d in range(2):
+                z_copy(hops[i - 1][d]).wait_recv()
+                z_copy(hops[i][d]).start()
+        for core, dy in fill[3 * i : 3 * (i + 1)] if i < 3 else fill[3 * 3 :]:
+            send_row(core, 1, dy)
+            send_row(core, NZ - 1, dy)
+
+    def dispatch(core):
+        for dy in range(NY):
+
+            @pl.loop(0, NZ - 2)
+            def _(i):
+                dz = beyond(i)
+                send_row(core, dz, dy)
+
     dispatch(0)
     dispatch(1)
 
@@ -241,7 +254,7 @@
         return remote(piece, piece, cs_sem.at[0], cr_sem.at[dy], partner, t)
 
     def start_y():
-        landed(kv.at[c, y, pl.ds(0, 5)], zr_sem.at[0])
+        landed(kv.at[c, y, 0], zr_sem.at[0])
         for stage in range(2):
             for d in range(2):
                 y_copy(d, stage).start()
@@ -552,7 +565,7 @@
             dma((4,)),
             dma((9,)),
             dma((1,)),
-            dma((3,)),
+            dma((7,)),
             dma((1,)),
             dma((4,)),
             dma((1,)),

time: 124 us -> 122 us (0.984)
  Pallas kernels: 120 us -> 117 us
    pallas_call x1, Pallas kernels: 120 us -> 117 us  [on_device(): pl.pallas_call(functools.partial(step_kernel, n_tp), name='step', out_sha...]
where the time goes in v5:
time: 122 us; the launch traced here: 121 us
  Pallas kernels  117 us (96%)
  local copies, waits for them, and re-layouts  3.53 us (3%)
    pallas_call x1, Pallas kernels, on_device(): pl.pallas_call(functools.partial(step_kernel, n_tp), name='step', out_sha...  117 us
    unnamed x2, local copies, waits for them, and re-layouts  3.53 us

profile of v5, /device:TPU:2, one launch (start us, length us, event | category | flops | bytes accessed | tf_op | source)
XLA Modules:
  0.0 121.2 jit_solution(2285030827177928180)
XLA Ops:
  0.6 117.0 %step.1 = (bf16[256,2,128]{2,1,0:T(2,128)(2,1)}, bf16[128,2048]{1,0:T(8,128)(2,1)}) custom-call(bf16[256,2,128]{2,1,0:T(2,128)(2,1)} %q_hbm.1, bf16[256,128]{1,0:T(8,128)(2,1)} %bitcast.7, bf16[256,128]{1,0:T(8,128)(2,1)} %bitcast.8, bf16[128,2048]{1,0:T(8,128)(2,1)} %rows_hbm.1, f32[64,2,4,128]{3,2,1,0:T(4,128)} %constant.4.clone.row_hbm, ...), custom_call_target="tpu_custom_call" | custom-call | tf_op jit(solution)/shard_map/step/pallas_call | solution.py:529
  117.7 1.7 %copy.18 = bf16[256,2,128]{2,1,0:T(2,128)(2,1)} copy(bf16[256,2,128]{2,1,0:T(2,128)(2,1)} %get-tuple-element.4) | data formatting | bytes 262144
  119.3 1.9 %copy.19 = bf16[128,2048]{1,0:T(8,128)(2,1)} copy(bf16[128,2048]{1,0:T(8,128)(2,1)} %get-tuple-element.5) | data formatting | bytes 1048576

commit v6 on v5

--- a/solution.py
+++ b/solution.py
@@ -30,11 +30,12 @@
 def step_kernel(
     n_tp,
     q_hbm, k_hbm, v_hbm, rows_hbm, row_hbm, col_hbm, gate_ref, up_ref, down_ref,
+    qg_hbm, kg_hbm, mg_hbm, ei_hbm, rw_hbm,
+    att_ref, comb_ref,
+    q_ref, k_ref, v_ref, rows_ref, row_ref, col_ref,
     qg_ref, kg_ref, mg_ref, ei_ref, rw_ref,
-    att_out, comb_out,
-    att_ref, comb_ref, q_ref, k_ref, v_ref, rows_ref, row_ref, col_ref,
     kv, wbuf, out, arr, arr16, total, hid, res, ret, qt, acc, stat, dmat, place,
-    in_sem, out_sem, loc_sem, own_sem, ws_sem, wr_sem, zs_sem, zr_sem, ys_sem, yr_sem, cs_sem, cr_sem,
+    in_sem, loc_sem, own_sem, ws_sem, wr_sem, zs_sem, zr_sem, ys_sem, yr_sem, cs_sem, cr_sem,
     ds_sem, dr_sem, rs_sem, rr_sem, go_sem,
 ):
     me = lax.axis_index("ep")
@@ -85,6 +86,7 @@
             (
                 (k_hbm, k_ref), (v_hbm, v_ref), (row_hbm.at[me], row_ref), (col_hbm, col_ref),
                 (rows_hbm, rows_ref), (q_hbm, q_ref),
+                (kg_hbm, kg_ref), (ei_hbm, ei_ref), (mg_hbm, mg_ref), (qg_hbm, qg_ref), (rw_hbm, rw_ref),
             )
         )
     ]
@@ -130,7 +132,7 @@
     for p in range(3):
         w_local(p).start()
 
-    for read in reads[:4]:
+    for read in reads[:4] + reads[6:8]:
         read.wait()
     length, width = k_ref.shape
     lines = row_ref.shape[1]
@@ -182,6 +184,7 @@
         z_copy(j).start()
 
     reads[4].wait()
+    reads[8].wait()
     arr16[0:rows_here, :] = rms(rows_ref[...].astype(F32), mg_ref[...]).astype(BF16)
 
     @pl.loop(0, n_ep * CAP // 128)
@@ -235,6 +238,7 @@
     dispatch(1)
 
     reads[5].wait()
+    reads[9].wait()
     q_f = q_ref[...].astype(F32)
     for h in range(q_ref.shape[1]):
         turned = turn(q_f[:, h, :], qg_ref[...])
@@ -315,7 +319,7 @@
 
     def last_part():
         last = (t + 2) % n_tp
-        per = step // CAP
+        per = step // CAP // 2
         landed(wbuf.at[0, pl.ds(0, 2)], wr_sem.at[7])
 
         @pl.loop(0, chunks)
@@ -325,29 +329,30 @@
 
         landed(wbuf.at[0, 2], wr_sem.at[8])
 
-        @pl.loop(0, chunks)
+        piece = step // 2
+
+        @pl.loop(0, 2 * chunks)
         def _(i):
-            at = pl.ds(i * step, step)
+            at = pl.ds(i * piece, piece)
             part = jnp.dot(hid[at, :], wbuf[last, 2], preferred_element_type=F32).astype(BF16).astype(F32)
             block = (total[at, :] + part).astype(BF16).astype(F32)
             res[pl.ds(i * per, per)] = block.reshape(per, CAP, model).astype(BF16)
 
-            core = (c + i) % NC
-
-            for dy in range(NY):
+            dc = i // 2
+            core = (c + dc) % NC
+
+            for pair in range(2):
+                dy = i % 2 * 2 + pair
 
                 @pl.loop(0, NZ)
                 def _(j):
                     dz = alternate(j)
-                    row = (z + NZ - dz) % NZ * NY + y_at[(NY - dy) % NY]
-                    k = i * plane + dy * NZ + dz
+                    row = (z + NZ - dz) % NZ * NY + (y + NY - dy) % NY
+                    k = dc * plane + dy * NZ + dz
                     copy = remote(
-                        res.at[k], ret.at[line(me)], rs_sem.at[0], rr_sem.at[i], row * NC + core, t
+                        res.at[k], ret.at[line(me)], rs_sem.at[0], rr_sem.at[dc], row * NC + core, t
                     )
-                    if dy > 0:
-                        copy.start()
-                    else:
-                        pl.when(k > 0)(copy.start)
+                    pl.when(k > 0)(copy.start)
 
         mine.start()
 
@@ -443,8 +448,6 @@
     done = acc[...] / stat[1:2, :]
     heads = [done[:, h * length : (h + 1) * length].T for h in range(cols // length)]
     att_ref[...] = jnp.stack(heads, axis=1).astype(BF16)
-    writes = [pltpu.make_async_copy(att_ref, att_out, out_sem.at[4])]
-    writes[0].start()
 
     sent(wbuf.at[pl.ds(0, 2)], ws_sem.at[3])
     sent(wbuf.at[0, 2], ws_sem.at[2])
@@ -453,6 +456,7 @@
     sent(kv.at[c], cs_sem.at[0])
     sent(out.at[pl.ds(0, n_ep - 1)], ds_sem.at[0])
 
+    reads[10].wait()
     weights = jnp.concatenate([rw_ref[...], pad], axis=0).T
     wide = 512
 
@@ -485,12 +489,8 @@
 
     sent(res.at[pl.ds(0, n_ep - 1)], rs_sem.at[0])
 
-    for i, (at, value) in enumerate(take(1)):
+    for at, value in take(1):
         comb_ref[:, at] = (total[0:rows_here, at] + value).astype(BF16)
-        writes.append(pltpu.make_async_copy(comb_ref.at[:, at], comb_out.at[:, at], out_sem.at[i]))
-        writes[-1].start()
-    for write in writes:
-        write.wait()
 
 
 def position_tables(count, width):
@@ -533,17 +533,20 @@
             jax.ShapeDtypeStruct((length, heads, width), BF16),
             jax.ShapeDtypeStruct((rows_here, model), BF16),
         ),
-        in_specs=[hbm] * 9 + [vmem] * 5,
-        out_specs=(hbm, hbm),
+        in_specs=[hbm] * 14,
+        out_specs=(vmem, vmem),
         scratch_shapes=[
-            pltpu.VMEM((length, heads, width), BF16),
-            pltpu.VMEM((rows_here, model), BF16),
             pltpu.VMEM((length, heads, width), BF16),
             pltpu.VMEM((length, width), BF16),
             pltpu.VMEM((length, width), BF16),
             pltpu.VMEM((rows_here, model), BF16),
             pltpu.VMEM((2, length // GRID_W, width), F32),
             pltpu.VMEM((2, GRID_W, width), F32),
+            pltpu.VMEM((1, width), F32),
+            pltpu.VMEM((1, width), F32),
+            pltpu.VMEM((1, model), F32),
+            pltpu.VMEM((2, rows_here), jnp.int32),
+            pltpu.VMEM((2, rows_here), F32),
             pltpu.VMEM((NC, NY, NZ, 2 * length, width), BF16),
             pltpu.VMEM((n_tp, 3, part, model), BF16),
             pltpu.VMEM((n_ep, CAP, model), BF16),
@@ -558,8 +561,7 @@
             pltpu.VMEM((8, heads * length), F32),
             pltpu.VMEM((slots, rows_here), BF16),
             pltpu.VMEM((2, rows_here, slots), BF16),
-            dma((6,)),
-            dma((5,)),
+            dma((11,)),
             dma((3,)),
             dma((2,)),
             dma((4,)),
@@ -577,13 +579,18 @@
             pltpu.SemaphoreType.REGULAR,
         ],
         compiler_params=pltpu.CompilerParams(
-            collective_id=0, has_side_effects=True, vmem_limit_bytes=60 * 1024 * 1024
+            collective_id=0, has_side_effects=True, vmem_limit_bytes=44 * 1024 * 1024
         ),
     )(
-        queries, keys.reshape(length, width), values.reshape(length, width),
-        routed_rows, rows, jnp.asarray(columns), expert_gate, expert_up, expert_down,
-        query_gain.reshape(1, width), key_gain.reshape(1, width), mixture_gain.reshape(1, model),
-        expert_index.T, route_weights.T,
+        *(
+            pltpu.with_memory_space_constraint(array, pltpu.HBM)
+            for array in (
+                queries, keys.reshape(length, width), values.reshape(length, width), routed_rows,
+                rows, jnp.asarray(columns), expert_gate, expert_up, expert_down,
+                query_gain.reshape(1, width), key_gain.reshape(1, width), mixture_gain.reshape(1, model),
+                expert_index.T, route_weights.T,
+            )
+        ),
     )
     return attended, combined
 

time: 122 us -> 119 us (0.975)
  local copies, waits for them, and re-layouts: 3.53 us -> 1.45 us
    unnamed x2, local copies, waits for them, and re-layouts: 3.53 us -> 1.45 us
    pallas_call x1, Pallas kernels: 117 us -> 116 us  [on_device(): pl.pallas_call(functools.partial(step_kernel, n_tp), name='step', out_sha...]
where the time goes in v6:
time: 119 us; the launch traced here: 118 us
  Pallas kernels  116 us (97%)
  local copies, waits for them, and re-layouts  1.45 us (1%)
    pallas_call x1, Pallas kernels, on_device(): pl.pallas_call(functools.partial(step_kernel, n_tp), name='step', out_sha...  116 us

profile of v6, /device:TPU:2, one launch (start us, length us, event | category | flops | bytes accessed | tf_op | source)
XLA Modules:
  0.0 117.7 jit_solution(3988139081949624201)
XLA Ops:
  0.6 115.6 %step.1 = (bf16[256,2,128]{2,1,0:T(2,128)(2,1)S(1)}, bf16[128,2048]{1,0:T(8,128)(2,1)S(1)}) custom-call(bf16[256,2,128]{2,1,0:T(2,128)(2,1)} %q_hbm.1, bf16[256,128]{1,0:T(8,128)(2,1)} %bitcast.7, bf16[256,128]{1,0:T(8,128)(2,1)} %bitcast.8, bf16[128,2048]{1,0:T(8,128)(2,1)} %rows_hbm.1, f32[64,2,4,128]{3,2,1,0:T(4,128)} %constant.4.clone.row_hbm, ...), custom_call_target="tpu_custom_call" | custom-call | tf_op jit(solution)/shard_map/step/pallas_call | solution.py:529
  116.3 0.7 copy.18
  116.9 0.8 copy.19

commit v7 on v6

--- a/solution.py
+++ b/solution.py
@@ -471,18 +471,12 @@
             landed(ret.at[pl.ds(core * plane, plane)], rr_sem.at[1])
 
         lines = plane * CAP
-        for i in range(lines // 128):
-            first = core * plane + i * (128 // CAP)
-            block = ret[first : first + 128 // CAP].astype(F32)
-            arr16[first * CAP : first * CAP + 128, :] = block.reshape(128, model).astype(BF16)
+        both = place[:, :, core * lines : (core + 1) * lines].reshape(2 * rows_here, lines)
         for j in range(model // wide):
-            block = arr16[core * lines : (core + 1) * lines, j * wide : (j + 1) * wide]
-            picked = [
-                jnp.dot(place[k, :, core * lines : (core + 1) * lines], block, preferred_element_type=F32)
-                * weights[:, k : k + 1]
-                for k in range(2)
-            ]
-            yield pl.ds(j * wide, wide), picked[0] + picked[1]
+            at = pl.ds(j * wide, wide)
+            block = ret[core * plane : (core + 1) * plane, :, at].astype(F32)
+            picked = jnp.dot(both, block.reshape(lines, wide).astype(BF16), preferred_element_type=F32)
+            yield at, picked[:rows_here] * weights[:, 0:1] + picked[rows_here:] * weights[:, 1:2]
 
     for at, value in take(0):
         total[0:rows_here, at] = value

time: 119 us -> 119 us (level)
  no operation moved by 1% of the time
where the time goes in v7:
time: 119 us; the launch traced here: 118 us
  Pallas kernels  116 us (97%)
  local copies, waits for them, and re-layouts  1.45 us (1%)
    pallas_call x1, Pallas kernels, on_device(): pl.pallas_call(functools.partial(step_kernel, n_tp), name='step', out_sha...  116 us

profile of v7, /device:TPU:2, one launch (start us, length us, event | category | flops | bytes accessed | tf_op | source)
XLA Modules:
  0.0 117.7 jit_solution(6090051957239306580)
XLA Ops:
  0.6 115.6 %step.1 = (bf16[256,2,128]{2,1,0:T(2,128)(2,1)S(1)}, bf16[128,2048]{1,0:T(8,128)(2,1)S(1)}) custom-call(bf16[256,2,128]{2,1,0:T(2,128)(2,1)} %q_hbm.1, bf16[256,128]{1,0:T(8,128)(2,1)} %bitcast.7, bf16[256,128]{1,0:T(8,128)(2,1)} %bitcast.8, bf16[128,2048]{1,0:T(8,128)(2,1)} %rows_hbm.1, f32[64,2,4,128]{3,2,1,0:T(4,128)} %constant.4.clone.row_hbm, ...), custom_call_target="tpu_custom_call" | custom-call | tf_op jit(solution)/shard_map/step/pallas_call | solution.py:523
  116.2 0.7 copy.18
  116.9 0.8 copy.19
